TPU v7x, 32 devices: a whole 2x2x4 slice. The times are simulated.
32 devices in a mesh: dp: 4 (over y, x), kv: 4 (over z), tp: 2 (over core).
Axes of the slice: x: 2, y: 2, z: 4, core: 2. Of those that a mesh axis runs over, the one named last changes fastest.
Arguments:
- tokens: bfloat16 [8192, 2048], P(('dp', 'kv')), parts along dimension 0, may hold values from -60 to 60, as said below
- chosen: int32 [128, 16], P(('dp', 'kv')), parts along dimension 0, may hold values from -1 to 31, as said below
- query_weight: bfloat16 [2048, 1024], P('kv', 'tp'), may hold values from -0.125 to 0.125
- key_matrix: bfloat16 [2048, 128], P('kv', 'tp'), may hold values from -0.125 to 0.125
- value_matrix: bfloat16 [2048, 128], P('kv', 'tp'), may hold values from -0.125 to 0.125
- out_weight: bfloat16 [1024, 2048], P('tp', 'kv'), may hold values from -0.1875 to 0.1875
- out_gain: float32 [2048], replicated, may hold values from 0.1 to 1.9
Outputs:
- mixed_out: bfloat16 [8192, 2048], P(('dp', 'kv', 'tp')), parts along dimension 0
There are 4 independent parts, one for each index of `dp`. A program takes and returns all parts, laid end to end along the dimension named above; an argument that names none is the same for every part. Nothing has to cross between parts.
Inputs may be any that keep to these rules, and one draw needn't show every extreme that they name: tokens are of order one apart from few rows. chosen[g, 0] = g; every other entry of row g is -1 or a block below g, and the entries of a row other than -1 are distinct; the blocks that the rows of one device name on any single other device are at most 2 different ones, and this is reached.
All inputs are finite; a program needn't handle non-finite values.
Results may differ from a plain program's by a relative error of at most 0.012.
The roundings to bfloat16 on the way count: a program that leaves them out, or rounds other values in their place, can miss the bound.
Values may be sent and summed in bfloat16 or wider, within the bound.
A program may use at most 64 MiB of HBM per device.

v0:
```python
import functools

import jax
import jax.numpy as jnp
from jax import lax
from jax.experimental import pallas as pl
from jax.experimental.pallas import tpu as pltpu
from jax.sharding import PartitionSpec as P

HEAD_WIDTH = 64
BLOCK_LENGTH = 64
LANES = 2 * HEAD_WIDTH
HIDDEN = -1e30
CAP = 2


def remote(src, dst, send, recv, axis, peer):
    return pltpu.make_async_remote_copy(
        src_ref=src,
        dst_ref=dst,
        send_sem=send,
        recv_sem=recv,
        device_id={axis: peer},
        device_id_type=pl.DeviceIdType.MESH,
    )


def fused(
    n_dp, n_kv, n_tp,
    chosen_hbm, tokens_hbm, key_hbm, value_hbm, query_hbm, out_hbm, gain_hbm, result,
    chosen, gain, tokens, pair_own, query_own, out_own, wanted, asks, packed, kv_own, kv_far,
    pair_all, query_all, out_all, kv_all, vk_all, query_sum, query_rows, attended,
    leaving, arriving, kept,
    load_sem, z_send, z_recv, d_send, d_recv, r_send, r_recv, kv_send, kv_recv, t_send, t_recv, ask_send, ask_recv,
):
    d, z, t = lax.axis_index("dp"), lax.axis_index("kv"), lax.axis_index("tp")
    rows, width = tokens.shape
    blocks = rows // BLOCK_LENGTH
    depth = width // n_kv
    half = rows // n_tp
    cut = depth // n_dp
    loads = [
        pltpu.make_async_copy(source, target, load_sem.at[k])
        for k, (source, target) in enumerate(
            ((query_hbm, query_own), (tokens_hbm, tokens), (out_hbm, out_own),
             (gain_hbm, gain), (chosen_hbm, wanted), (chosen_hbm, chosen))
        )
    ]
    pair_loads = [
        pltpu.make_async_copy(
            source.at[:, k * cut : (k + 1) * cut],
            pair_own.at[k, side * HEAD_WIDTH : (side + 1) * HEAD_WIDTH],
            load_sem.at[6 + k * 2 + side],
        )
        for k in range(n_dp)
        for side, source in enumerate((key_hbm, value_hbm))
    ]
    for load in pair_loads + loads:
        load.start()

    barrier = pltpu.get_barrier_semaphore()
    for axis, me, count in (("dp", d, n_dp), ("kv", z, n_kv), ("tp", t, n_tp)):
        for step in range(1, count):
            pl.semaphore_signal(
                barrier, inc=1, device_id={axis: lax.rem(me + step, count)},
                device_id_type=pl.DeviceIdType.MESH,
            )
    pl.semaphore_wait(barrier, n_dp + n_kv + n_tp - 3)

    owns = (pair_own, query_own, out_own)
    alls = (pair_all, query_all, out_all)

    def first(which, j):
        return remote(
            owns[which].at[d], alls[which].at[z, d], z_send.at[which, j], z_recv.at[which, j],
            "kv", lax.rem(z + j, n_kv),
        )

    def first_in(which, j):
        slot = alls[which].at[lax.rem(z + n_kv - j, n_kv), d]
        return remote(
            slot, slot, z_send.at[which, j], z_recv.at[which, j], "kv", lax.rem(z + j, n_kv)
        )

    near = (d, d + 1 - 2 * lax.rem(d, 2), lax.rem(d + 2, 4))
    corner = 3 - d

    def second(which, j, k, place=None):
        slot = alls[which].at[lax.rem(z + n_kv - j, n_kv), d if place is None else place]
        return remote(
            slot, slot, d_send.at[which, j, k], d_recv.at[which, j, k], "dp", near[k]
        )

    def halfway(which, j, k, place):
        rows_half = owns[which].shape[1] // 2
        slot = alls[which].at[
            lax.rem(z + n_kv - j, n_kv), place, (k - 1) * rows_half : k * rows_half
        ]
        return remote(
            slot, slot, r_send.at[which, j, k], r_recv.at[which, j, k], "dp", near[3 - k]
        )

    def relay(which, j):
        for k in (1, 2):
            second(which, j, k, near[k]).wait_recv()
            halfway(which, j, k, near[k]).start()

    def pass_on(which, j):
        first_in(which, j).wait_recv()
        for k in (1, 2):
            second(which, j, k).start()

    def take(which, j):
        if j:
            for k in (1, 2):
                halfway(which, j, k, corner).wait_recv()

    def whole(which, j):
        block = owns[which][...] if j == 0 else alls[which][lax.rem(z + n_kv - j, n_kv)]
        return block.reshape(block.shape[0] * block.shape[1], block.shape[2])

    def token_part(j):
        start = pl.multiple_of(lax.rem(z + n_kv - j, n_kv) * depth, depth)
        return tokens[:, pl.ds(start, depth)]

    def ask(j):
        return remote(
            wanted, asks.at[z], ask_send.at[j], ask_recv.at[j], "kv", lax.rem(z + n_kv - j, n_kv)
        )

    def ask_in(j):
        slot = asks.at[lax.rem(z + j, n_kv)]
        return remote(
            slot, slot, ask_send.at[j], ask_recv.at[j], "kv", lax.rem(z + n_kv - j, n_kv)
        )

    loads[4].wait()
    for j in range(1, n_kv):
        ask(j).start()
    for which in (0, 1):
        for load in (pair_loads, loads[:1])[which]:
            load.wait()
        for j in range(1, n_kv):
            first(which, j).start()
    for j in range(1, n_kv):
        pass_on(0, j)
    for j in range(1, n_kv):
        pass_on(1, j)
        if j == 1:
            for k in range(1, n_kv):
                relay(0, k)
        elif j < n_kv - 1:
            relay(1, j - 1)
    for load in loads[1:4] + loads[5:]:
        load.wait()

    def pair_part(j):
        block = pair_own[...] if j == 0 else pair_all[lax.rem(z + n_kv - j, n_kv)]
        block = jnp.concatenate([block[k] for k in range(n_dp)], axis=1)
        return lax.dot_general(
            token_part(j), block, (((1,), (1,)), ((), ())), preferred_element_type=jnp.float32
        )

    total = pair_part(0)
    for j in range(1, n_kv):
        take(0, j)
        total += pair_part(j)
    kv_own[...] = total.astype(jnp.bfloat16).reshape(blocks, BLOCK_LENGTH, LANES)

    def named(rows_of, owner):
        local = rows_of - owner * blocks
        inside = (local >= 0) & (local < blocks)
        return (
            jnp.min(jnp.where(inside, local, blocks - 1)),
            jnp.max(jnp.where(inside, local, 0)),
        )

    def kv_out(j):
        return remote(
            packed.at[j], kv_far.at[pl.ds(z * CAP, CAP)], kv_send.at[j], kv_recv.at[j],
            "kv", lax.rem(z + j, n_kv),
        )

    def kv_in(j):
        slot = kv_far.at[pl.ds(lax.rem(z + n_kv - j, n_kv) * CAP, CAP)]
        return remote(slot, slot, kv_send.at[j], kv_recv.at[j], "kv", lax.rem(z + j, n_kv))

    kv_far[pl.ds(z * CAP, CAP)] = jnp.zeros((CAP, BLOCK_LENGTH, LANES), jnp.bfloat16)
    for j in range(1, n_kv):
        ask_in(j).wait_recv()
        lowest, highest = named(asks[lax.rem(z + j, n_kv)], z)
        packed[j, 0] = kv_own[lowest]
        packed[j, 1] = kv_own[highest]
    firsts = [named(wanted[...], owner)[0] + owner * blocks for owner in range(n_kv)]
    for j in range(1, n_kv):
        kv_out(j).start()
    for j in range(max(n_kv - 2, 1), n_kv):
        relay(1, j)
    for j in range(1, n_kv):
        first(2, j).start()

    query_sum[...] = jnp.dot(token_part(0), whole(1, 0), preferred_element_type=jnp.float32)
    for j in range(1, n_kv):
        take(1, j)
        query_sum[...] += jnp.dot(token_part(j), whole(1, j), preferred_element_type=jnp.float32)
    query_rows[...] = query_sum[...].astype(jnp.bfloat16) * jnp.bfloat16(HEAD_WIDTH ** (-0.5))

    for j in range(1, n_kv):
        kv_in(j).wait_recv()

    swap = (
        lax.rem(lax.broadcasted_iota(jnp.int32, (LANES, LANES), 0) + HEAD_WIDTH, LANES)
        == lax.broadcasted_iota(jnp.int32, (LANES, LANES), 1)
    ).astype(jnp.float32).astype(jnp.bfloat16)
    for source, start in ((kv_far, 0), (kv_own, n_kv * CAP)):
        count = source.shape[0]
        part = source[...]
        turned = jnp.dot(
            part.reshape(count * BLOCK_LENGTH, LANES), swap, preferred_element_type=jnp.float32
        )
        kv_all[start : start + count] = part
        vk_all[start : start + count] = turned.astype(jnp.bfloat16).reshape(part.shape)

    picks = chosen.shape[1]
    pairs = query_rows.shape[1] // LANES

    def attend(b, carry):
        for j in range(1, n_kv):

            @pl.when(b == min(j, blocks - 1))
            def _(j=j):
                pass_on(2, j)

            @pl.when(b == min(j + 4, blocks - 1))
            def _(j=j):
                relay(2, j)

        lane = lax.broadcasted_iota(jnp.int32, (BLOCK_LENGTH, LANES), 1)
        row = lax.broadcasted_iota(jnp.int32, (BLOCK_LENGTH, LANES), 0)
        low = (lane < HEAD_WIDTH).astype(jnp.float32)
        names = [chosen[b, s] for s in range(picks)]
        offs = [jnp.where(name >= 0, 0.0, HIDDEN) for name in names]
        bias = []
        for s in range(0, picks, 2):
            tile = jnp.where(lane < HEAD_WIDTH, offs[s], offs[s + 1])
            if s == 0:
                tile = jnp.where((lane < HEAD_WIDTH) & (lane > row), HIDDEN, tile)
            bias.append(tile)
        bias = jnp.concatenate(bias, axis=1)

        def place(name):
            name = jnp.maximum(name, 0)
            spot = name - z * blocks + n_kv * CAP
            for owner in range(n_kv):
                local = name - owner * blocks
                away = (local >= 0) & (local < blocks) & (z != owner)
                far = owner * CAP + jnp.where(name == firsts[owner], 0, 1)
                spot = jnp.where(away, far, spot)
            return spot

        safe = [jnp.where(name >= 0, place(name), 0) for name in names]
        kv = jnp.concatenate([kv_all[g] for g in safe], axis=0)
        vk = jnp.concatenate([vk_all[g] for g in safe], axis=0)
        at = pl.ds(pl.multiple_of(b * BLOCK_LENGTH, BLOCK_LENGTH), BLOCK_LENGTH)
        query = query_rows[at, :]
        stacked = jnp.concatenate(
            [query[:, p * LANES : (p + 1) * LANES] for p in range(pairs)], axis=0
        )
        keep = jnp.concatenate([low] * pairs, axis=0)
        outs = []
        for side in range(2):
            mask = keep if side == 0 else 1.0 - keep
            masked = stacked * mask.astype(jnp.bfloat16)
            keys, values = (kv, vk) if side == 0 else (vk, kv)
            scores = lax.dot_general(
                masked, keys, (((1,), (1,)), ((), ())), preferred_element_type=jnp.float32
            )
            scores = scores.reshape(pairs, BLOCK_LENGTH, picks * BLOCK_LENGTH) + bias[None]
            top = jnp.max(scores, axis=2, keepdims=True)
            expon = jnp.exp(scores - top)
            inverse = 1.0 / jnp.sum(expon, axis=2, keepdims=True)
            probs = expon.astype(jnp.bfloat16)
            probs = probs.reshape(pairs * BLOCK_LENGTH, picks * BLOCK_LENGTH)
            out = jnp.dot(probs, values, preferred_element_type=jnp.float32)
            outs.append(out * inverse.reshape(pairs * BLOCK_LENGTH, 1))
        joined = jnp.where(keep > 0.5, outs[0], outs[1]).astype(jnp.bfloat16)
        for p in range(pairs):
            attended[at, p * LANES : (p + 1) * LANES] = joined[
                p * BLOCK_LENGTH : (p + 1) * BLOCK_LENGTH
            ]
        return carry

    lax.fori_loop(0, blocks, attend, 0)

    peer = lax.rem(t + 1, n_tp)
    other_rows = attended[pl.ds(pl.multiple_of(peer * half, half), half), :]
    own_rows = attended[pl.ds(pl.multiple_of(t * half, half), half), :]

    def swap_half(j):
        slot = lax.rem(z + n_kv - j, n_kv)
        return remote(
            leaving.at[slot], arriving.at[slot], t_send.at[j], t_recv.at[j], "tp", peer
        )

    for j in range(n_kv):
        take(2, j)
        weight = whole(2, j)
        slot = lax.rem(z + n_kv - j, n_kv)
        leaving[slot] = jnp.dot(
            other_rows, weight, preferred_element_type=jnp.float32
        ).astype(jnp.bfloat16)
        swap_half(j).start()
        kept[slot] = jnp.dot(own_rows, weight, preferred_element_type=jnp.float32)

    square = jnp.zeros((half, 1), jnp.float32)
    for j in range(n_kv):
        slot = lax.rem(z + n_kv - j, n_kv)
        swap_half(j).wait_recv()
        mixed = kept[slot] + arriving[slot].astype(jnp.float32)
        kept[slot] = mixed
        square += jnp.sum(mixed * mixed, axis=1, keepdims=True)
    scale = lax.rsqrt(square * (1.0 / width) + 1e-06)
    for j in range(n_kv):
        columns = slice(j * depth, (j + 1) * depth)
        result[:, columns] = (kept[j] * scale * gain[:, columns]).astype(jnp.bfloat16)

    for which in range(3):
        for j in range(1, n_kv):
            first(which, j).wait_send()
            for k in (1, 2):
                second(which, j, k).wait_send()
                halfway(which, j, k, near[k]).wait_send()
    for j in range(1, n_kv):
        kv_out(j).wait_send()
        ask(j).wait_send()
    for j in range(n_kv):
        swap_half(j).wait_send()


def per_device_fused(
    n_dp, n_kv, n_tp,
    tokens, chosen, query_weight, key_matrix, value_matrix, out_weight, out_gain,
):
    rows, width = tokens.shape
    depth, columns = query_weight.shape
    blocks = rows // BLOCK_LENGTH
    cut = lambda w: w.reshape(n_dp, w.shape[0] // n_dp, w.shape[1])
    query, out = cut(query_weight), cut(out_weight)
    pair = jax.ShapeDtypeStruct((n_dp, LANES, depth // n_dp), jnp.bfloat16)
    bf16, f32 = jnp.bfloat16, jnp.float32
    vmem = pl.BlockSpec(memory_space=pltpu.VMEM)
    off_core = pl.BlockSpec(memory_space=pltpu.HBM)
    dma = pltpu.SemaphoreType.DMA
    return pl.pallas_call(
        functools.partial(fused, n_dp, n_kv, n_tp),
        out_shape=jax.ShapeDtypeStruct((rows // n_tp, width), bf16),
        in_specs=[
            off_core, off_core, off_core, off_core, off_core, off_core, off_core,
        ],
        out_specs=vmem,
        scratch_shapes=[
            pltpu.SMEM((blocks, chosen.shape[1]), jnp.int32),
            pltpu.VMEM((1, width), f32),
            pltpu.VMEM((rows, width), bf16),
            pltpu.VMEM(pair.shape, bf16),
            pltpu.VMEM(query.shape, bf16),
            pltpu.VMEM(out.shape, bf16),
            pltpu.VMEM((blocks, chosen.shape[1]), jnp.int32),
            pltpu.VMEM((n_kv, blocks, chosen.shape[1]), jnp.int32),
            pltpu.VMEM((n_kv, CAP, BLOCK_LENGTH, LANES), bf16),
            pltpu.VMEM((blocks, BLOCK_LENGTH, LANES), bf16),
            pltpu.VMEM((n_kv * CAP, BLOCK_LENGTH, LANES), bf16),
            pltpu.VMEM((n_kv,) + pair.shape, bf16),
            pltpu.VMEM((n_kv,) + query.shape, bf16),
            pltpu.VMEM((n_kv,) + out.shape, bf16),
            pltpu.VMEM((n_kv * CAP + blocks, BLOCK_LENGTH, LANES), bf16),
            pltpu.VMEM((n_kv * CAP + blocks, BLOCK_LENGTH, LANES), bf16),
            pltpu.VMEM((rows, columns), f32),
            pltpu.VMEM((rows, columns), bf16),
            pltpu.VMEM((rows, columns), bf16),
            pltpu.VMEM((n_kv, rows // n_tp, width // n_kv), bf16),
            pltpu.VMEM((n_kv, rows // n_tp, width // n_kv), bf16),
            pltpu.VMEM((n_kv, rows // n_tp, width // n_kv), f32),
            dma((6 + 2 * n_dp,)), dma((3, n_kv)), dma((3, n_kv)), dma((3, n_kv, 3)), dma((3, n_kv, 3)),
            dma((3, n_kv, 3)), dma((3, n_kv, 3)),
            dma((n_kv,)), dma((n_kv,)), dma((n_kv,)), dma((n_kv,)),
            dma((n_kv,)), dma((n_kv,)),
        ],
        compiler_params=pltpu.CompilerParams(
            collective_id=0, has_side_effects=True, vmem_limit_bytes=54 * 1024 * 1024
        ),
    )(chosen, tokens, key_matrix.T, value_matrix.T, query, out, out_gain.reshape(1, width))


def per_device(tokens, chosen, query_weight, key_matrix, value_matrix, out_weight, out_gain):
    tok_rows = tokens.shape[0]
    blocks = tok_rows // BLOCK_LENGTH
    device = lax.axis_index("kv")
    kv_count = lax.axis_size("kv")
    whole_query, whole_key, whole_value = (
        lax.all_gather(query_weight, "kv", axis=0, tiled=True),
        lax.all_gather(key_matrix, "kv", axis=0, tiled=True),
        lax.all_gather(value_matrix, "kv", axis=0, tiled=True),
    )
    query_rows = jnp.dot(tokens, whole_query, preferred_element_type=jnp.float32).astype(
        jnp.bfloat16
    )
    key_rows = jnp.dot(tokens, whole_key, preferred_element_type=jnp.float32).astype(jnp.bfloat16)
    value_rows = jnp.dot(tokens, whole_value, preferred_element_type=jnp.float32).astype(
        jnp.bfloat16
    )
    paired = jnp.concatenate([key_rows, value_rows], axis=1)
    pair_width = paired.shape[1]
    safe_ids = jnp.maximum(chosen, 0)
    everyone = lax.all_gather(paired, "kv", axis=0, tiled=True).reshape(
        kv_count * blocks, BLOCK_LENGTH, pair_width
    )
    picked = jnp.take(everyone, safe_ids, axis=0)
    head_count = query_rows.shape[1] // HEAD_WIDTH
    grouped = query_rows.reshape(blocks, BLOCK_LENGTH, head_count, HEAD_WIDTH)
    offsets = jnp.arange(BLOCK_LENGTH, dtype=jnp.int32)
    query_pos = (device * blocks + jnp.arange(blocks, dtype=jnp.int32))[
        :, None
    ] * BLOCK_LENGTH + offsets[None, :]
    key_pos = safe_ids[:, :, None] * BLOCK_LENGTH + offsets[None, None, :]
    visible = (chosen >= 0)[:, None, :, None] & (
        key_pos[:, None, :, :] <= query_pos[:, :, None, None]
    )

    def attend_block(inputs):
        query_block, pair_block, seen = inputs
        block_keys = pair_block[..., :HEAD_WIDTH]
        block_values = pair_block[..., HEAD_WIDTH:]
        scores = jnp.einsum(
            "qgd,skd->gqsk", query_block, block_keys, preferred_element_type=jnp.float32
        ) * HEAD_WIDTH ** (-0.5)
        scores = jnp.where(seen[None], scores, -1e30)
        row_max = jnp.max(scores, axis=(2, 3), keepdims=True)
        expon = jnp.exp(scores - row_max)
        row_sum = jnp.sum(expon, axis=(2, 3), keepdims=True)
        weights_bf = (expon / row_sum).astype(jnp.bfloat16)
        result = jnp.einsum(
            "gqsk,skd->qgd", weights_bf, block_values, preferred_element_type=jnp.float32
        )
        return result.astype(jnp.bfloat16)

    attended = lax.map(attend_block, (grouped, picked, visible))
    attended = attended.reshape(tok_rows, head_count * HEAD_WIDTH)
    whole_out = lax.all_gather(out_weight, "kv", axis=1, tiled=True)
    mixed = lax.psum_scatter(
        jnp.dot(attended, whole_out, preferred_element_type=jnp.float32).astype(jnp.bfloat16),
        "tp",
        scatter_dimension=0,
        tiled=True,
    ).astype(jnp.float32)
    normed = mixed * lax.rsqrt(jnp.mean(mixed * mixed, axis=-1, keepdims=True) + 1e-06) * out_gain
    return normed.astype(jnp.bfloat16)


def solution(mesh):
    placed = (
        P(("dp", "kv"), None),
        P(("dp", "kv"), None),
        P("kv", "tp"),
        P("kv", "tp"),
        P("kv", "tp"),
        P("tp", "kv"),
        P(),
    )
    n_dp, n_kv, n_tp = (mesh.shape[name] for name in ("dp", "kv", "tp"))

    def body(tokens, chosen, query_weight, key_matrix, value_matrix, out_weight, out_gain):
        args = (tokens, chosen, query_weight, key_matrix, value_matrix, out_weight, out_gain)
        depth, columns = query_weight.shape
        whole_tiles = (
            depth % (LANES * n_dp) == 0
            and out_weight.shape[0] % (16 * n_dp) == 0
            and out_weight.shape[1] % LANES == 0
            and columns % LANES == 0
            and key_matrix.shape[1] == HEAD_WIDTH
            and chosen.shape[1] % 2 == 0
            and n_tp == 2
            and n_dp == 4
        )
        if whole_tiles:
            return per_device_fused(n_dp, n_kv, n_tp, *args)
        return per_device(*args)

    return jax.shard_map(
        body,
        mesh=mesh,
        in_specs=placed,
        out_specs=P(("dp", "kv", "tp"), None),
        check_vma=False,
    )
```

profile of v0, /device:TPU:1, one launch (start us, length us, event | category | flops | bytes accessed | tf_op | source)
XLA Modules:
  0.0 55.4 jit_solution(6420760823686496147)
XLA Ops:
  0.0 53.1 %shard_map.73 = bf16[256,2048]{1,0:T(8,128)(2,1)} custom-call(s32[8,16]{1,0:T(8,128)} %chosen_hbm.1, bf16[512,2048]{1,0:T(8,128)(2,1)} %tokens_hbm.1, bf16[64,512]{1,0:T(8,128)(2,1)} %bitcast.7, bf16[64,512]{1,0:T(8,128)(2,1)} %bitcast.8, bf16[4,128,512]{2,1,0:T(8,128)(2,1)} %bitcast.5, bf16[4,128,512]{2,1,0:T(8,128)(2,1)} %bitcast.6, f32[1,2048]{1,0:T(1,128)} %bitcast.9), custom_call_target="tpu_custom_call" | custom-call | tf_op jit(solution)/shard_map/pallas_call | solution.py:354
  53.1 2.3 %copy.9 = bf16[256,2048]{1,0:T(8,128)(2,1)} copy(bf16[256,2048]{1,0:T(8,128)(2,1)} %shard_map.73) | data formatting | bytes 2097152
where the time goes:
time: 55.5 us; the launch traced here: 55.4 us
  Pallas kernels  53.1 us (96%)
  local copies, waits for them, and re-layouts  2.3 us (4%)
    pallas_call x1, Pallas kernels, per_device_fused(): pl.pallas_call(functools.partial(fused, n_dp, n_kv, n_tp), out_shape=jax....  53.1 us
    unnamed x1, local copies, waits for them, and re-layouts  2.3 us

commit v1 on v0

--- a/solution.py
+++ b/solution.py
@@ -12,6 +12,7 @@
 LANES = 2 * HEAD_WIDTH
 HIDDEN = -1e30
 CAP = 2
+PIECES = (1, 2, 2)
 
 
 def remote(src, dst, send, recv, axis, peer):
@@ -31,7 +32,7 @@
     chosen, gain, tokens, pair_own, query_own, out_own, wanted, asks, packed, kv_own, kv_far,
     pair_all, query_all, out_all, kv_all, vk_all, query_sum, query_rows, attended,
     leaving, arriving, kept,
-    load_sem, z_send, z_recv, d_send, d_recv, r_send, r_recv, kv_send, kv_recv, t_send, t_recv, ask_send, ask_recv,
+    load_sem, z_send, z_recv, f_send, d_send, d_recv, r_send, r_recv, kv_send, kv_recv, t_send, t_recv, ask_send, ask_recv,
 ):
     d, z, t = lax.axis_index("dp"), lax.axis_index("kv"), lax.axis_index("tp")
     rows, width = tokens.shape
@@ -69,93 +70,129 @@
 
     owns = (pair_own, query_own, out_own)
     alls = (pair_all, query_all, out_all)
-
-    def first(which, j):
-        return remote(
-            owns[which].at[d], alls[which].at[z, d], z_send.at[which, j], z_recv.at[which, j],
-            "kv", lax.rem(z + j, n_kv),
-        )
-
-    def first_in(which, j):
-        slot = alls[which].at[lax.rem(z + n_kv - j, n_kv), d]
-        return remote(
-            slot, slot, z_send.at[which, j], z_recv.at[which, j], "kv", lax.rem(z + j, n_kv)
-        )
-
+    events = [
+        (which, part, j) for which in range(3) for part in range(PIECES[which]) for j in range(1, n_kv)
+    ]
+    origin = (z, z + 1 - 2 * lax.rem(z, 2), lax.rem(z + 2, 4), 3 - z)
+    middle = (z == 1) | (z == 2)
     near = (d, d + 1 - 2 * lax.rem(d, 2), lax.rem(d + 2, 4))
     corner = 3 - d
 
-    def second(which, j, k, place=None):
-        slot = alls[which].at[lax.rem(z + n_kv - j, n_kv), d if place is None else place]
+    def span_of(e, share=0, shares=1):
+        which, part, _ = events[e]
+        size = owns[which].shape[1] // PIECES[which]
+        return pl.ds(part * size + share * (size // shares), size // shares)
+
+    def first(e):
+        which, _, j = events[e]
         return remote(
-            slot, slot, d_send.at[which, j, k], d_recv.at[which, j, k], "dp", near[k]
-        )
-
-    def halfway(which, j, k, place):
-        rows_half = owns[which].shape[1] // 2
-        slot = alls[which].at[
-            lax.rem(z + n_kv - j, n_kv), place, (k - 1) * rows_half : k * rows_half
-        ]
-        return remote(
-            slot, slot, r_send.at[which, j, k], r_recv.at[which, j, k], "dp", near[3 - k]
-        )
-
-    def relay(which, j):
+            owns[which].at[d, span_of(e)], alls[which].at[z, d, span_of(e)],
+            z_send.at[e], z_recv.at[e], "kv", origin[j],
+        )
+
+    def first_in(e):
+        which, _, j = events[e]
+        slot = alls[which].at[origin[j], d, span_of(e)]
+        return remote(slot, slot, z_send.at[e], z_recv.at[e], "kv", origin[j])
+
+    def onward(e):
+        which, _, j = events[e]
+        slot = alls[which].at[origin[j], d, span_of(e)]
+        return remote(slot, slot, f_send.at[e], z_recv.at[e + 1], "kv", origin[1])
+
+    def second(e, k, place=None):
+        which, _, j = events[e]
+        slot = alls[which].at[origin[j], d if place is None else place, span_of(e)]
+        return remote(slot, slot, d_send.at[e, k], d_recv.at[e, k], "dp", near[k])
+
+    def halfway(e, k, place):
+        which, _, j = events[e]
+        slot = alls[which].at[origin[j], place, span_of(e, k - 1, 2)]
+        return remote(slot, slot, r_send.at[e, k], r_recv.at[e, k], "dp", near[3 - k])
+
+    def out(e):
+        if events[e][2] == 3:
+
+            @pl.when(middle)
+            def _():
+                first(e).start()
+        else:
+            first(e).start()
+
+    def pass_on(e):
+        first_in(e).wait_recv()
+        if events[e][2] == 2:
+
+            @pl.when(middle)
+            def _():
+                onward(e).start()
+
         for k in (1, 2):
-            second(which, j, k, near[k]).wait_recv()
-            halfway(which, j, k, near[k]).start()
-
-    def pass_on(which, j):
-        first_in(which, j).wait_recv()
+            second(e, k).start()
+
+    def relay(e):
         for k in (1, 2):
-            second(which, j, k).start()
-
-    def take(which, j):
-        if j:
-            for k in (1, 2):
-                halfway(which, j, k, corner).wait_recv()
+            second(e, k, near[k]).wait_recv()
+            halfway(e, k, near[k]).start()
+
+    def take(e):
+        for k in (1, 2):
+            halfway(e, k, corner).wait_recv()
 
     def whole(which, j):
-        block = owns[which][...] if j == 0 else alls[which][lax.rem(z + n_kv - j, n_kv)]
+        block = owns[which][...] if j == 0 else alls[which][origin[j]]
         return block.reshape(block.shape[0] * block.shape[1], block.shape[2])
 
     def token_part(j):
-        start = pl.multiple_of(lax.rem(z + n_kv - j, n_kv) * depth, depth)
+        start = pl.multiple_of(origin[j] * depth, depth)
         return tokens[:, pl.ds(start, depth)]
 
     def ask(j):
-        return remote(
-            wanted, asks.at[z], ask_send.at[j], ask_recv.at[j], "kv", lax.rem(z + n_kv - j, n_kv)
-        )
+        return remote(wanted, asks.at[z], ask_send.at[j], ask_recv.at[j], "kv", origin[j])
 
     def ask_in(j):
-        slot = asks.at[lax.rem(z + j, n_kv)]
-        return remote(
-            slot, slot, ask_send.at[j], ask_recv.at[j], "kv", lax.rem(z + n_kv - j, n_kv)
-        )
+        slot = asks.at[origin[j]]
+        return remote(slot, slot, ask_send.at[j], ask_recv.at[j], "kv", origin[j])
 
     loads[4].wait()
     for j in range(1, n_kv):
         ask(j).start()
-    for which in (0, 1):
-        for load in (pair_loads, loads[:1])[which]:
-            load.wait()
-        for j in range(1, n_kv):
-            first(which, j).start()
-    for j in range(1, n_kv):
-        pass_on(0, j)
-    for j in range(1, n_kv):
-        pass_on(1, j)
-        if j == 1:
-            for k in range(1, n_kv):
-                relay(0, k)
-        elif j < n_kv - 1:
-            relay(1, j - 1)
-    for load in loads[1:4] + loads[5:]:
+    for load in pair_loads:
         load.wait()
+    for e in (1, 0):
+        out(e)
+    loads[0].wait()
+    for e in (3, 4):
+        out(e)
+    pass_on(0)
+    out(2)
+    pass_on(1)
+    out(7)
+    pass_on(3)
+    for e in (6, 5, 8):
+        out(e)
+    loads[2].wait()
+    out(13)
+    relay(0)
+    pass_on(2)
+    relay(1)
+    pass_on(4)
+    out(10)
+    relay(3)
+    out(9)
+    take(0)
+    relay(2)
+    for e in (7, 6):
+        pass_on(e)
+    take(1)
+    out(12)
+    take(2)
+    pass_on(5)
+    for load in loads[1:2] + loads[3:4] + loads[5:]:
+        load.wait()
 
     def pair_part(j):
-        block = pair_own[...] if j == 0 else pair_all[lax.rem(z + n_kv - j, n_kv)]
+        block = pair_own[...] if j == 0 else pair_all[origin[j]]
         block = jnp.concatenate([block[k] for k in range(n_dp)], axis=1)
         return lax.dot_general(
             token_part(j), block, (((1,), (1,)), ((), ())), preferred_element_type=jnp.float32
@@ -163,7 +200,6 @@
 
     total = pair_part(0)
     for j in range(1, n_kv):
-        take(0, j)
         total += pair_part(j)
     kv_own[...] = total.astype(jnp.bfloat16).reshape(blocks, BLOCK_LENGTH, LANES)
 
@@ -178,33 +214,50 @@
     def kv_out(j):
         return remote(
             packed.at[j], kv_far.at[pl.ds(z * CAP, CAP)], kv_send.at[j], kv_recv.at[j],
-            "kv", lax.rem(z + j, n_kv),
+            "kv", origin[j],
         )
 
     def kv_in(j):
-        slot = kv_far.at[pl.ds(lax.rem(z + n_kv - j, n_kv) * CAP, CAP)]
-        return remote(slot, slot, kv_send.at[j], kv_recv.at[j], "kv", lax.rem(z + j, n_kv))
+        slot = kv_far.at[pl.ds(origin[j] * CAP, CAP)]
+        return remote(slot, slot, kv_send.at[j], kv_recv.at[j], "kv", origin[j])
 
     kv_far[pl.ds(z * CAP, CAP)] = jnp.zeros((CAP, BLOCK_LENGTH, LANES), jnp.bfloat16)
     for j in range(1, n_kv):
         ask_in(j).wait_recv()
-        lowest, highest = named(asks[lax.rem(z + j, n_kv)], z)
+        lowest, highest = named(asks[origin[j]], z)
         packed[j, 0] = kv_own[lowest]
         packed[j, 1] = kv_own[highest]
     firsts = [named(wanted[...], owner)[0] + owner * blocks for owner in range(n_kv)]
+    pass_on(8)
+    for e in (7, 6):
+        relay(e)
     for j in range(1, n_kv):
         kv_out(j).start()
-    for j in range(max(n_kv - 2, 1), n_kv):
-        relay(1, j)
-    for j in range(1, n_kv):
-        first(2, j).start()
-
+    relay(4)
+    take(3)
+    relay(5)
     query_sum[...] = jnp.dot(token_part(0), whole(1, 0), preferred_element_type=jnp.float32)
-    for j in range(1, n_kv):
-        take(1, j)
-        query_sum[...] += jnp.dot(token_part(j), whole(1, j), preferred_element_type=jnp.float32)
+    relay(8)
+    take(7)
+    for e in (13, 9, 12):
+        pass_on(e)
+    out(14)
+    take(6)
+    out(11)
+    take(4)
+    query_sum[...] += jnp.dot(
+        token_part(1), whole(1, 1), preferred_element_type=jnp.float32
+    )
+    pass_on(10)
+    take(5)
+    query_sum[...] += jnp.dot(
+        token_part(2), whole(1, 2), preferred_element_type=jnp.float32
+    )
+    take(8)
+    query_sum[...] += jnp.dot(
+        token_part(3), whole(1, 3), preferred_element_type=jnp.float32
+    )
     query_rows[...] = query_sum[...].astype(jnp.bfloat16) * jnp.bfloat16(HEAD_WIDTH ** (-0.5))
-
     for j in range(1, n_kv):
         kv_in(j).wait_recv()
 
@@ -221,19 +274,30 @@
         kv_all[start : start + count] = part
         vk_all[start : start + count] = turned.astype(jnp.bfloat16).reshape(part.shape)
 
+    pass_on(14)
+
     picks = chosen.shape[1]
     pairs = query_rows.shape[1] // LANES
 
     def attend(b, carry):
-        for j in range(1, n_kv):
-
-            @pl.when(b == min(j, blocks - 1))
-            def _(j=j):
-                pass_on(2, j)
-
-            @pl.when(b == min(j + 4, blocks - 1))
-            def _(j=j):
-                relay(2, j)
+        @pl.when(b == 2)
+        def _():
+            pass_on(11)
+            relay(9)
+
+        @pl.when(b == 4)
+        def _():
+            for e in (12, 13):
+                relay(e)
+
+        @pl.when(b == 5)
+        def _():
+            for e in (14, 10):
+                relay(e)
+
+        @pl.when(b == 6)
+        def _():
+            relay(11)
 
         lane = lax.broadcasted_iota(jnp.int32, (BLOCK_LENGTH, LANES), 1)
         row = lax.broadcasted_iota(jnp.int32, (BLOCK_LENGTH, LANES), 0)
@@ -297,24 +361,32 @@
     own_rows = attended[pl.ds(pl.multiple_of(t * half, half), half), :]
 
     def swap_half(j):
-        slot = lax.rem(z + n_kv - j, n_kv)
         return remote(
-            leaving.at[slot], arriving.at[slot], t_send.at[j], t_recv.at[j], "tp", peer
-        )
-
-    for j in range(n_kv):
-        take(2, j)
+            leaving.at[origin[j]], arriving.at[origin[j]], t_send.at[j], t_recv.at[j], "tp", peer
+        )
+
+    def project(j):
         weight = whole(2, j)
-        slot = lax.rem(z + n_kv - j, n_kv)
-        leaving[slot] = jnp.dot(
+        leaving[origin[j]] = jnp.dot(
             other_rows, weight, preferred_element_type=jnp.float32
         ).astype(jnp.bfloat16)
         swap_half(j).start()
-        kept[slot] = jnp.dot(own_rows, weight, preferred_element_type=jnp.float32)
+        kept[origin[j]] = jnp.dot(own_rows, weight, preferred_element_type=jnp.float32)
+
+    for e in (13, 9):
+        take(e)
+    project(0)
+    take(12)
+    project(1)
+    take(10)
+    project(2)
+    for e in (11, 14):
+        take(e)
+    project(3)
 
     square = jnp.zeros((half, 1), jnp.float32)
     for j in range(n_kv):
-        slot = lax.rem(z + n_kv - j, n_kv)
+        slot = origin[j]
         swap_half(j).wait_recv()
         mixed = kept[slot] + arriving[slot].astype(jnp.float32)
         kept[slot] = mixed
@@ -324,12 +396,21 @@
         columns = slice(j * depth, (j + 1) * depth)
         result[:, columns] = (kept[j] * scale * gain[:, columns]).astype(jnp.bfloat16)
 
-    for which in range(3):
-        for j in range(1, n_kv):
-            first(which, j).wait_send()
-            for k in (1, 2):
-                second(which, j, k).wait_send()
-                halfway(which, j, k, near[k]).wait_send()
+    for e in range(len(events)):
+        if events[e][2] < 3:
+            first(e).wait_send()
+        for k in (1, 2):
+            second(e, k).wait_send()
+            halfway(e, k, near[k]).wait_send()
+
+    @pl.when(middle)
+    def _():
+        for e in range(len(events)):
+            if events[e][2] == 3:
+                first(e).wait_send()
+            if events[e][2] == 2:
+                onward(e).wait_send()
+
     for j in range(1, n_kv):
         kv_out(j).wait_send()
         ask(j).wait_send()
@@ -351,9 +432,10 @@
     vmem = pl.BlockSpec(memory_space=pltpu.VMEM)
     off_core = pl.BlockSpec(memory_space=pltpu.HBM)
     dma = pltpu.SemaphoreType.DMA
+    copies = sum(PIECES) * (n_kv - 1)
     return pl.pallas_call(
         functools.partial(fused, n_dp, n_kv, n_tp),
-        out_shape=jax.ShapeDtypeStruct((rows // n_tp, width), bf16),
+        out_shape=pltpu.VMEM((rows // n_tp, width), bf16),
         in_specs=[
             off_core, off_core, off_core, off_core, off_core, off_core, off_core,
         ],
@@ -381,8 +463,8 @@
             pltpu.VMEM((n_kv, rows // n_tp, width // n_kv), bf16),
             pltpu.VMEM((n_kv, rows // n_tp, width // n_kv), bf16),
             pltpu.VMEM((n_kv, rows // n_tp, width // n_kv), f32),
-            dma((6 + 2 * n_dp,)), dma((3, n_kv)), dma((3, n_kv)), dma((3, n_kv, 3)), dma((3, n_kv, 3)),
-            dma((3, n_kv, 3)), dma((3, n_kv, 3)),
+            dma((6 + 2 * n_dp,)), dma((copies,)), dma((copies,)), dma((copies,)),
+            dma((copies, 3)), dma((copies, 3)), dma((copies, 3)), dma((copies, 3)),
             dma((n_kv,)), dma((n_kv,)), dma((n_kv,)), dma((n_kv,)),
             dma((n_kv,)), dma((n_kv,)),
         ],
@@ -474,13 +556,16 @@
         depth, columns = query_weight.shape
         whole_tiles = (
             depth % (LANES * n_dp) == 0
-            and out_weight.shape[0] % (16 * n_dp) == 0
+            and depth % (32 * PIECES[1] * n_dp) == 0
+            and out_weight.shape[0] % (32 * PIECES[2] * n_dp) == 0
             and out_weight.shape[1] % LANES == 0
             and columns % LANES == 0
             and key_matrix.shape[1] == HEAD_WIDTH
             and chosen.shape[1] % 2 == 0
             and n_tp == 2
             and n_dp == 4
+            and n_kv == 4
+            and tokens.shape[0] == 8 * BLOCK_LENGTH
         )
         if whole_tiles:
             return per_device_fused(n_dp, n_kv, n_tp, *args)

time: 55.5 us -> 49.1 us (0.88)
  Pallas kernels: 53.1 us -> 47.9 us
  local copies, waits for them, and re-layouts: 2.3 us -> 0.97 us
    pallas_call x1, Pallas kernels: 53.1 us -> 47.9 us  [per_device_fused(): pl.pallas_call(functools.partial(fused, n_dp, n_kv, n_tp), out_shape=pltp...]
    unnamed x1, local copies, waits for them, and re-layouts: 2.3 us -> 0.97 us
where the time goes in v1:
time: 49.1 us; the launch traced here: 48.9 us
  Pallas kernels  47.9 us (98%)
  local copies, waits for them, and re-layouts  0.97 us (2%)
    pallas_call x1, Pallas kernels, per_device_fused(): pl.pallas_call(functools.partial(fused, n_dp, n_kv, n_tp), out_shape=pltp...  47.9 us

profile of v1, /device:TPU:1, one launch (start us, length us, event | category | flops | bytes accessed | tf_op | source)
XLA Modules:
  0.0 48.9 jit_solution(17389087959741504041)
XLA Ops:
  0.0 47.9 %shard_map.73 = bf16[256,2048]{1,0:T(8,128)(2,1)S(1)} custom-call(s32[8,16]{1,0:T(8,128)} %chosen_hbm.1, bf16[512,2048]{1,0:T(8,128)(2,1)} %tokens_hbm.1, bf16[64,512]{1,0:T(8,128)(2,1)} %bitcast.7, bf16[64,512]{1,0:T(8,128)(2,1)} %bitcast.8, bf16[4,128,512]{2,1,0:T(8,128)(2,1)} %bitcast.5, bf16[4,128,512]{2,1,0:T(8,128)(2,1)} %bitcast.6, f32[1,2048]{1,0:T(1,128)} %bitcast.9), custom_call_target="tpu_custom_call" | custom-call | tf_op jit(solution)/shard_map/pallas_call | solution.py:436
  47.9 1.0 %copy.9 = bf16[256,2048]{1,0:T(8,128)(2,1)} copy(bf16[256,2048]{1,0:T(8,128)(2,1)S(1)} %shard_map.73) | data formatting | bytes 2097152

commit v2 on v1

--- a/solution.py
+++ b/solution.py
@@ -29,10 +29,10 @@
 def fused(
     n_dp, n_kv, n_tp,
     chosen_hbm, tokens_hbm, key_hbm, value_hbm, query_hbm, out_hbm, gain_hbm, result,
-    chosen, gain, tokens, pair_own, query_own, out_own, wanted, asks, packed, kv_own, kv_far,
-    pair_all, query_all, out_all, kv_all, vk_all, query_sum, query_rows, attended,
+    chosen, spots, lowest_of, gain, tokens, pair_own, query_own, out_own, wanted, asks, packed, kv_own, kv_far,
+    pair_all, query_all, out_all, kv_all, query_sum, query_rows, attended,
     leaving, arriving, kept,
-    load_sem, z_send, z_recv, f_send, d_send, d_recv, r_send, r_recv, kv_send, kv_recv, t_send, t_recv, ask_send, ask_recv,
+    load_sem, z_send, z_recv, d_send, d_recv, r_send, r_recv, kv_send, kv_recv, t_send, t_recv, ask_send, ask_recv,
 ):
     d, z, t = lax.axis_index("dp"), lax.axis_index("kv"), lax.axis_index("tp")
     rows, width = tokens.shape
@@ -51,7 +51,7 @@
         pltpu.make_async_copy(
             source.at[:, k * cut : (k + 1) * cut],
             pair_own.at[k, side * HEAD_WIDTH : (side + 1) * HEAD_WIDTH],
-            load_sem.at[6 + k * 2 + side],
+            load_sem.at[6],
         )
         for k in range(n_dp)
         for side, source in enumerate((key_hbm, value_hbm))
@@ -87,28 +87,38 @@
         which, _, j = events[e]
         return remote(
             owns[which].at[d, span_of(e)], alls[which].at[z, d, span_of(e)],
-            z_send.at[e], z_recv.at[e], "kv", origin[j],
+            z_send.at[which], z_recv.at[e], "kv", origin[j],
         )
 
     def first_in(e):
         which, _, j = events[e]
         slot = alls[which].at[origin[j], d, span_of(e)]
-        return remote(slot, slot, z_send.at[e], z_recv.at[e], "kv", origin[j])
+        return remote(slot, slot, z_send.at[which], z_recv.at[e], "kv", origin[j])
 
     def onward(e):
         which, _, j = events[e]
         slot = alls[which].at[origin[j], d, span_of(e)]
-        return remote(slot, slot, f_send.at[e], z_recv.at[e + 1], "kv", origin[1])
-
-    def second(e, k, place=None):
-        which, _, j = events[e]
-        slot = alls[which].at[origin[j], d if place is None else place, span_of(e)]
-        return remote(slot, slot, d_send.at[e, k], d_recv.at[e, k], "dp", near[k])
-
-    def halfway(e, k, place):
-        which, _, j = events[e]
-        slot = alls[which].at[origin[j], place, span_of(e, k - 1, 2)]
-        return remote(slot, slot, r_send.at[e, k], r_recv.at[e, k], "dp", near[3 - k])
+        return remote(slot, slot, z_send.at[which], z_recv.at[e + 1], "kv", origin[1])
+
+    def second(e, k):
+        which, _, j = events[e]
+        slot = alls[which].at[origin[j], d, span_of(e)]
+        return remote(slot, slot, d_send.at[which], d_recv.at[e], "dp", near[k])
+
+    def second_in(e):
+        which, _, j = events[e]
+        slots = alls[which].at[origin[j], 0:2, span_of(e)]
+        return remote(slots, slots, d_send.at[which], d_recv.at[e], "dp", near[1])
+
+    def halfway(e, k):
+        which, _, j = events[e]
+        slot = alls[which].at[origin[j], near[k], span_of(e, k - 1, 2)]
+        return remote(slot, slot, r_send.at[which], r_recv.at[e], "dp", near[3 - k])
+
+    def halfway_in(e):
+        which, _, j = events[e]
+        slot = alls[which].at[origin[j], corner, span_of(e)]
+        return remote(slot, slot, r_send.at[which], r_recv.at[e], "dp", near[1])
 
     def out(e):
         if events[e][2] == 3:
@@ -131,13 +141,12 @@
             second(e, k).start()
 
     def relay(e):
+        second_in(e).wait_recv()
         for k in (1, 2):
-            second(e, k, near[k]).wait_recv()
-            halfway(e, k, near[k]).start()
+            halfway(e, k).start()
 
     def take(e):
-        for k in (1, 2):
-            halfway(e, k, corner).wait_recv()
+        halfway_in(e).wait_recv()
 
     def whole(which, j):
         block = owns[which][...] if j == 0 else alls[which][origin[j]]
@@ -148,17 +157,16 @@
         return tokens[:, pl.ds(start, depth)]
 
     def ask(j):
-        return remote(wanted, asks.at[z], ask_send.at[j], ask_recv.at[j], "kv", origin[j])
-
-    def ask_in(j):
-        slot = asks.at[origin[j]]
-        return remote(slot, slot, ask_send.at[j], ask_recv.at[j], "kv", origin[j])
+        return remote(wanted, asks.at[z], ask_send.at[0], ask_recv.at[0], "kv", origin[j])
+
+    def asks_in():
+        slots = asks.at[0 : n_kv - 1]
+        return remote(slots, slots, ask_send.at[0], ask_recv.at[0], "kv", origin[1])
 
     loads[4].wait()
     for j in range(1, n_kv):
         ask(j).start()
-    for load in pair_loads:
-        load.wait()
+    pltpu.make_async_copy(pair_own, pair_own, load_sem.at[6]).wait()
     for e in (1, 0):
         out(e)
     loads[0].wait()
@@ -213,26 +221,38 @@
 
     def kv_out(j):
         return remote(
-            packed.at[j], kv_far.at[pl.ds(z * CAP, CAP)], kv_send.at[j], kv_recv.at[j],
+            packed.at[j], kv_far.at[pl.ds(z * CAP, CAP)], kv_send.at[0], kv_recv.at[0],
             "kv", origin[j],
         )
 
-    def kv_in(j):
-        slot = kv_far.at[pl.ds(origin[j] * CAP, CAP)]
-        return remote(slot, slot, kv_send.at[j], kv_recv.at[j], "kv", origin[j])
+    def kv_in():
+        slots = kv_far.at[0 : (n_kv - 1) * CAP]
+        return remote(slots, slots, kv_send.at[0], kv_recv.at[0], "kv", origin[1])
 
     kv_far[pl.ds(z * CAP, CAP)] = jnp.zeros((CAP, BLOCK_LENGTH, LANES), jnp.bfloat16)
+    asks_in().wait_recv()
     for j in range(1, n_kv):
-        ask_in(j).wait_recv()
         lowest, highest = named(asks[origin[j]], z)
         packed[j, 0] = kv_own[lowest]
         packed[j, 1] = kv_own[highest]
-    firsts = [named(wanted[...], owner)[0] + owner * blocks for owner in range(n_kv)]
+    picks = chosen.shape[1]
+    for owner in range(n_kv):
+        lowest_of[owner] = named(wanted[...], owner)[0] + owner * blocks
     pass_on(8)
     for e in (7, 6):
         relay(e)
     for j in range(1, n_kv):
         kv_out(j).start()
+
+    def locate(b, carry):
+        for s in range(picks):
+            name = jnp.maximum(chosen[b, s], 0)
+            owner = lax.div(name, blocks)
+            far = owner * CAP + jnp.where(name == lowest_of[owner], 0, 1)
+            spots[b, s] = jnp.where(owner == z, name - z * blocks + n_kv * CAP, far)
+        return carry
+
+    lax.fori_loop(0, blocks, locate, 0)
     relay(4)
     take(3)
     relay(5)
@@ -257,27 +277,21 @@
     query_sum[...] += jnp.dot(
         token_part(3), whole(1, 3), preferred_element_type=jnp.float32
     )
-    query_rows[...] = query_sum[...].astype(jnp.bfloat16) * jnp.bfloat16(HEAD_WIDTH ** (-0.5))
-    for j in range(1, n_kv):
-        kv_in(j).wait_recv()
-
-    swap = (
-        lax.rem(lax.broadcasted_iota(jnp.int32, (LANES, LANES), 0) + HEAD_WIDTH, LANES)
-        == lax.broadcasted_iota(jnp.int32, (LANES, LANES), 1)
-    ).astype(jnp.float32).astype(jnp.bfloat16)
-    for source, start in ((kv_far, 0), (kv_own, n_kv * CAP)):
-        count = source.shape[0]
-        part = source[...]
-        turned = jnp.dot(
-            part.reshape(count * BLOCK_LENGTH, LANES), swap, preferred_element_type=jnp.float32
-        )
-        kv_all[start : start + count] = part
-        vk_all[start : start + count] = turned.astype(jnp.bfloat16).reshape(part.shape)
+    low_half = lax.broadcasted_iota(jnp.int32, (rows, LANES), 1) < HEAD_WIDTH
+    for p in range(query_sum.shape[1] // LANES):
+        both = query_sum[:, p * LANES : (p + 1) * LANES]
+        for side, one in enumerate((both, pltpu.roll(both, HEAD_WIDTH, 1))):
+            one = jnp.where(low_half, one, 0.0).astype(jnp.bfloat16)
+            query_rows[2 * p + side] = one * jnp.bfloat16(HEAD_WIDTH ** (-0.5))
+    kv_in().wait_recv()
+
+    kv_all[0 : n_kv * CAP] = kv_far[...]
+    kv_all[n_kv * CAP :] = kv_own[...]
 
     pass_on(14)
 
-    picks = chosen.shape[1]
-    pairs = query_rows.shape[1] // LANES
+    heads = query_rows.shape[0]
+    group = heads // 2
 
     def attend(b, carry):
         @pl.when(b == 2)
@@ -301,57 +315,40 @@
 
         lane = lax.broadcasted_iota(jnp.int32, (BLOCK_LENGTH, LANES), 1)
         row = lax.broadcasted_iota(jnp.int32, (BLOCK_LENGTH, LANES), 0)
-        low = (lane < HEAD_WIDTH).astype(jnp.float32)
-        names = [chosen[b, s] for s in range(picks)]
-        offs = [jnp.where(name >= 0, 0.0, HIDDEN) for name in names]
+        low = lane < HEAD_WIDTH
+        offs = [jnp.where(chosen[b, s] >= 0, 0.0, HIDDEN) for s in range(picks)]
         bias = []
         for s in range(0, picks, 2):
-            tile = jnp.where(lane < HEAD_WIDTH, offs[s], offs[s + 1])
+            tile = jnp.where(low, offs[s], offs[s + 1])
             if s == 0:
-                tile = jnp.where((lane < HEAD_WIDTH) & (lane > row), HIDDEN, tile)
+                tile = jnp.where(low & (lane > row), HIDDEN, tile)
             bias.append(tile)
         bias = jnp.concatenate(bias, axis=1)
-
-        def place(name):
-            name = jnp.maximum(name, 0)
-            spot = name - z * blocks + n_kv * CAP
-            for owner in range(n_kv):
-                local = name - owner * blocks
-                away = (local >= 0) & (local < blocks) & (z != owner)
-                far = owner * CAP + jnp.where(name == firsts[owner], 0, 1)
-                spot = jnp.where(away, far, spot)
-            return spot
-
-        safe = [jnp.where(name >= 0, place(name), 0) for name in names]
-        kv = jnp.concatenate([kv_all[g] for g in safe], axis=0)
-        vk = jnp.concatenate([vk_all[g] for g in safe], axis=0)
+        kv = jnp.concatenate([kv_all[spots[b, s]] for s in range(picks)], axis=0)
         at = pl.ds(pl.multiple_of(b * BLOCK_LENGTH, BLOCK_LENGTH), BLOCK_LENGTH)
-        query = query_rows[at, :]
-        stacked = jnp.concatenate(
-            [query[:, p * LANES : (p + 1) * LANES] for p in range(pairs)], axis=0
-        )
-        keep = jnp.concatenate([low] * pairs, axis=0)
+
+        def score(start):
+            query = query_rows[start : start + group, at, :].reshape(group * BLOCK_LENGTH, LANES)
+            return lax.dot_general(
+                query, kv, (((1,), (1,)), ((), ())), preferred_element_type=jnp.float32
+            )
+
         outs = []
-        for side in range(2):
-            mask = keep if side == 0 else 1.0 - keep
-            masked = stacked * mask.astype(jnp.bfloat16)
-            keys, values = (kv, vk) if side == 0 else (vk, kv)
-            scores = lax.dot_general(
-                masked, keys, (((1,), (1,)), ((), ())), preferred_element_type=jnp.float32
-            )
-            scores = scores.reshape(pairs, BLOCK_LENGTH, picks * BLOCK_LENGTH) + bias[None]
+        later = score(0)
+        for start in range(0, heads, group):
+            scores = later.reshape(group, BLOCK_LENGTH, picks * BLOCK_LENGTH) + bias[None]
+            if start + group < heads:
+                later = score(start + group)
             top = jnp.max(scores, axis=2, keepdims=True)
             expon = jnp.exp(scores - top)
             inverse = 1.0 / jnp.sum(expon, axis=2, keepdims=True)
-            probs = expon.astype(jnp.bfloat16)
-            probs = probs.reshape(pairs * BLOCK_LENGTH, picks * BLOCK_LENGTH)
-            out = jnp.dot(probs, values, preferred_element_type=jnp.float32)
-            outs.append(out * inverse.reshape(pairs * BLOCK_LENGTH, 1))
-        joined = jnp.where(keep > 0.5, outs[0], outs[1]).astype(jnp.bfloat16)
-        for p in range(pairs):
-            attended[at, p * LANES : (p + 1) * LANES] = joined[
-                p * BLOCK_LENGTH : (p + 1) * BLOCK_LENGTH
-            ]
+            probs = expon.astype(jnp.bfloat16).reshape(group * BLOCK_LENGTH, picks * BLOCK_LENGTH)
+            out_rows = jnp.dot(probs, kv, preferred_element_type=jnp.float32)
+            out_rows = out_rows.reshape(group, BLOCK_LENGTH, LANES) * inverse
+            outs += [out_rows[h] for h in range(group)]
+        for p in range(heads // 2):
+            joined = jnp.where(low, pltpu.roll(outs[2 * p], HEAD_WIDTH, 1), outs[2 * p + 1])
+            attended[at, p * LANES : (p + 1) * LANES] = joined.astype(jnp.bfloat16)
         return carry
 
     lax.fori_loop(0, blocks, attend, 0)
@@ -362,7 +359,7 @@
 
     def swap_half(j):
         return remote(
-            leaving.at[origin[j]], arriving.at[origin[j]], t_send.at[j], t_recv.at[j], "tp", peer
+            leaving.at[origin[j]], arriving.at[origin[j]], t_send.at[0], t_recv.at[j], "tp", peer
         )
 
     def project(j):
@@ -396,26 +393,26 @@
         columns = slice(j * depth, (j + 1) * depth)
         result[:, columns] = (kept[j] * scale * gain[:, columns]).astype(jnp.bfloat16)
 
-    for e in range(len(events)):
-        if events[e][2] < 3:
-            first(e).wait_send()
-        for k in (1, 2):
-            second(e, k).wait_send()
-            halfway(e, k, near[k]).wait_send()
+    def drain(slots, sem):
+        remote(slots, slots, sem, z_recv.at[0], "kv", origin[1]).wait_send()
+
+    for which in range(3):
+        drain(alls[which].at[0 : n_kv - 1, 0:2], d_send.at[which])
+        drain(alls[which].at[0 : n_kv - 1, 0], r_send.at[which])
 
     @pl.when(middle)
     def _():
-        for e in range(len(events)):
-            if events[e][2] == 3:
-                first(e).wait_send()
-            if events[e][2] == 2:
-                onward(e).wait_send()
-
-    for j in range(1, n_kv):
-        kv_out(j).wait_send()
-        ask(j).wait_send()
-    for j in range(n_kv):
-        swap_half(j).wait_send()
+        for which in range(3):
+            drain(alls[which].at[:, 0], z_send.at[which])
+
+    @pl.when(jnp.logical_not(middle))
+    def _():
+        for which in range(3):
+            drain(alls[which].at[0:2, 0], z_send.at[which])
+
+    drain(packed.at[1:n_kv], kv_send.at[0])
+    drain(asks.at[0 : n_kv - 1], ask_send.at[0])
+    drain(leaving, t_send.at[0])
 
 
 def per_device_fused(
@@ -442,6 +439,8 @@
         out_specs=vmem,
         scratch_shapes=[
             pltpu.SMEM((blocks, chosen.shape[1]), jnp.int32),
+            pltpu.SMEM((blocks, chosen.shape[1]), jnp.int32),
+            pltpu.SMEM((n_kv,), jnp.int32),
             pltpu.VMEM((1, width), f32),
             pltpu.VMEM((rows, width), bf16),
             pltpu.VMEM(pair.shape, bf16),
@@ -456,17 +455,14 @@
             pltpu.VMEM((n_kv,) + query.shape, bf16),
             pltpu.VMEM((n_kv,) + out.shape, bf16),
             pltpu.VMEM((n_kv * CAP + blocks, BLOCK_LENGTH, LANES), bf16),
-            pltpu.VMEM((n_kv * CAP + blocks, BLOCK_LENGTH, LANES), bf16),
             pltpu.VMEM((rows, columns), f32),
-            pltpu.VMEM((rows, columns), bf16),
+            pltpu.VMEM((columns // HEAD_WIDTH, rows, LANES), bf16),
             pltpu.VMEM((rows, columns), bf16),
             pltpu.VMEM((n_kv, rows // n_tp, width // n_kv), bf16),
             pltpu.VMEM((n_kv, rows // n_tp, width // n_kv), bf16),
             pltpu.VMEM((n_kv, rows // n_tp, width // n_kv), f32),
-            dma((6 + 2 * n_dp,)), dma((copies,)), dma((copies,)), dma((copies,)),
-            dma((copies, 3)), dma((copies, 3)), dma((copies, 3)), dma((copies, 3)),
-            dma((n_kv,)), dma((n_kv,)), dma((n_kv,)), dma((n_kv,)),
-            dma((n_kv,)), dma((n_kv,)),
+            dma((7,)), dma((3,)), dma((copies,)), dma((3,)), dma((copies,)), dma((3,)), dma((copies,)),
+            dma((1,)), dma((1,)), dma((1,)), dma((n_kv,)), dma((1,)), dma((1,)),
         ],
         compiler_params=pltpu.CompilerParams(
             collective_id=0, has_side_effects=True, vmem_limit_bytes=54 * 1024 * 1024

time: 49.1 us -> 45.3 us (0.923)
  Pallas kernels: 47.9 us -> 44.2 us
    pallas_call x1, Pallas kernels: 47.9 us -> 44.2 us  [per_device_fused(): pl.pallas_call(functools.partial(fused, n_dp, n_kv, n_tp), out_shape=pltp...]
where the time goes in v2:
time: 45.3 us; the launch traced here: 45.2 us
  Pallas kernels  44.2 us (98%)
  local copies, waits for them, and re-layouts  0.97 us (2%)
    pallas_call x1, Pallas kernels, per_device_fused(): pl.pallas_call(functools.partial(fused, n_dp, n_kv, n_tp), out_shape=pltp...  44.2 us
    unnamed x1, local copies, waits for them, and re-layouts  0.97 us

profile of v2, /device:TPU:1, one launch (start us, length us, event | category | flops | bytes accessed | tf_op | source)
XLA Modules:
  0.0 45.2 jit_solution(16588418291306890092)
XLA Ops:
  0.0 44.2 %shard_map.73 = bf16[256,2048]{1,0:T(8,128)(2,1)S(1)} custom-call(s32[8,16]{1,0:T(8,128)} %chosen_hbm.1, bf16[512,2048]{1,0:T(8,128)(2,1)} %tokens_hbm.1, bf16[64,512]{1,0:T(8,128)(2,1)} %bitcast.7, bf16[64,512]{1,0:T(8,128)(2,1)} %bitcast.8, bf16[4,128,512]{2,1,0:T(8,128)(2,1)} %bitcast.5, bf16[4,128,512]{2,1,0:T(8,128)(2,1)} %bitcast.6, f32[1,2048]{1,0:T(1,128)} %bitcast.9), custom_call_target="tpu_custom_call" | custom-call | tf_op jit(solution)/shard_map/pallas_call | solution.py:433
  44.2 1.0 %copy.9 = bf16[256,2048]{1,0:T(8,128)(2,1)} copy(bf16[256,2048]{1,0:T(8,128)(2,1)S(1)} %shard_map.73) | data formatting | bytes 2097152

commit v3 on v2

v3 whole, which is shorter than its diff:
```python
import functools

import jax
import jax.numpy as jnp
from jax import lax
from jax.experimental import pallas as pl
from jax.experimental.pallas import tpu as pltpu
from jax.sharding import PartitionSpec as P

HEAD_WIDTH = 64
BLOCK_LENGTH = 64
LANES = 2 * HEAD_WIDTH
HIDDEN = -1e30
CAP = 2
PIECES = (1, 2, 2)
FAR = 1


def remote(src, dst, send, recv, axis, peer):
    return pltpu.make_async_remote_copy(
        src_ref=src,
        dst_ref=dst,
        send_sem=send,
        recv_sem=recv,
        device_id={axis: peer},
        device_id_type=pl.DeviceIdType.MESH,
    )


def fused(
    n_dp, n_kv, n_tp,
    chosen_hbm, tokens_hbm, key_hbm, value_hbm, query_hbm, out_hbm, gain_hbm, result,
    chosen, spots, lowest_of, gain, tokens, pair_own, query_own, out_own, wanted, asks, packed, kv_own, kv_far,
    pair_all, query_all, out_all, kv_all, query_sum, query_rows, attended,
    leaving, arriving, kept,
    load_sem, z_send, z_recv, c_send, c_recv, d_send, d_recv, r_send, r_recv, kv_send, kv_recv, t_send, t_recv, ask_send, ask_recv,
):
    d, z, t = lax.axis_index("dp"), lax.axis_index("kv"), lax.axis_index("tp")
    rows, width = tokens.shape
    blocks = rows // BLOCK_LENGTH
    depth = width // n_kv
    half = rows // n_tp
    cut = depth // n_dp
    loads = [
        pltpu.make_async_copy(source, target, load_sem.at[k])
        for k, (source, target) in enumerate(
            ((tokens_hbm, tokens), (out_hbm, out_own), (gain_hbm, gain), (chosen_hbm, wanted),
             (chosen_hbm, chosen))
        )
    ]
    part_width = query_own.shape[3]
    query_loads = [
        pltpu.make_async_copy(
            query_hbm.at[:, :, part * part_width : (part + 1) * part_width], query_own.at[part],
            load_sem.at[6 + part],
        )
        for part in range(PIECES[1])
    ]
    pair_loads = [
        pltpu.make_async_copy(
            source.at[:, k * cut : (k + 1) * cut],
            pair_own.at[k, side * HEAD_WIDTH : (side + 1) * HEAD_WIDTH],
            load_sem.at[5],
        )
        for k in range(n_dp)
        for side, source in enumerate((key_hbm, value_hbm))
    ]
    for load in pair_loads + loads[3:4] + query_loads + loads[:3] + loads[4:]:
        load.start()

    barrier = pltpu.get_barrier_semaphore()
    for axis, me, count in (("dp", d, n_dp), ("kv", z, n_kv), ("tp", t, n_tp)):
        for step in range(1, count):
            pl.semaphore_signal(
                barrier, inc=1, device_id={axis: lax.rem(me + step, count)},
                device_id_type=pl.DeviceIdType.MESH,
            )
    pl.semaphore_wait(barrier, n_dp + n_kv + n_tp - 3)

    owns = (pair_own, query_own, out_own)
    alls = (pair_all, query_all, out_all)
    events = [
        (which, part, j) for which in range(3) for part in range(PIECES[which]) for j in range(1, n_kv)
    ]
    far = [e for e, event in enumerate(events) if event[0] == 2 and event[1] >= PIECES[2] - FAR]
    origin = (z, z + 1 - 2 * lax.rem(z, 2), lax.rem(z + 2, 4), 3 - z)
    middle = (z == 1) | (z == 2)
    near = (d, d + 1 - 2 * lax.rem(d, 2), lax.rem(d + 2, 4))
    corner = 3 - d

    def piece_of(e, planes, plane, quarter, share=0, shares=1):
        which, part, _ = events[e]
        lead = (plane,) if planes else ()
        refs = alls if planes else owns
        if which == 1:
            size = refs[which].shape[-2] // shares
            return refs[which].at[(*lead, part, quarter, pl.ds(share * size, size))]
        size = refs[which].shape[-2] // PIECES[which]
        span = pl.ds(part * size + share * (size // shares), size // shares)
        return refs[which].at[(*lead, quarter, span)]

    def slot(e, quarter, share=0, shares=1):
        return piece_of(e, True, origin[events[e][2]], quarter, share, shares)

    def across(e, quarter, send, recv):
        return remote(
            piece_of(e, False, None, quarter), piece_of(e, True, z, quarter), send, recv,
            "kv", origin[events[e][2]],
        )

    def first(e):
        return across(e, d, z_send.at[events[e][0]], z_recv.at[e])

    def first_far(e):
        return across(e, corner, c_send.at[0], c_recv.at[far.index(e)])

    def landed(e, quarter, recv):
        place = slot(e, quarter)
        return remote(place, place, c_send.at[0], recv, "kv", origin[1])

    def onward(e):
        place = slot(e, d)
        return remote(place, place, z_send.at[events[e][0]], z_recv.at[e + 1], "kv", origin[1])

    def onward_far(e):
        place = slot(e, corner)
        return remote(
            place, place, c_send.at[0], c_recv.at[far.index(e) + 1], "kv", origin[1]
        )

    def second(e, k):
        place = slot(e, d)
        return remote(place, place, d_send.at[events[e][0]], d_recv.at[e], "dp", near[k])

    def second_in(e):
        places = slot(e, pl.ds(0, 2))
        return remote(places, places, d_send.at[events[e][0]], d_recv.at[e], "dp", near[1])

    def halfway(e, k):
        place = slot(e, near[k], k - 1, 2)
        return remote(place, place, r_send.at[events[e][0]], r_recv.at[e], "dp", near[3 - k])

    def halfway_in(e):
        place = slot(e, corner)
        return remote(place, place, r_send.at[events[e][0]], r_recv.at[e], "dp", near[1])

    def begin(copy, e):
        if events[e][2] == 3:

            @pl.when(middle)
            def _():
                copy(e).start()
        else:
            copy(e).start()

    def hand_on(copy, e):
        if events[e][2] == 2:

            @pl.when(middle)
            def _():
                copy(e).start()

    def out(e):
        begin(first, e)

    def out_far(e):
        begin(first_far, e)

    def pass_on(e):
        landed(e, d, z_recv.at[e]).wait_recv()
        hand_on(onward, e)
        for k in (1, 2):
            second(e, k).start()

    def pass_far(e):
        landed(e, corner, c_recv.at[far.index(e)]).wait_recv()
        hand_on(onward_far, e)

    def relay(e):
        second_in(e).wait_recv()
        if e not in far:
            for k in (1, 2):
                halfway(e, k).start()

    def take(e):
        halfway_in(e).wait_recv()

    def whole(which, j, part=None):
        block = owns[which] if j == 0 else alls[which].at[origin[j]]
        block = block[...] if part is None else block[part]
        return block.reshape(block.shape[0] * block.shape[1], block.shape[2])

    def token_part(j):
        start = pl.multiple_of(origin[j] * depth, depth)
        return tokens[:, pl.ds(start, depth)]

    def ask(j):
        return remote(wanted, asks.at[z], ask_send.at[0], ask_recv.at[0], "kv", origin[j])

    def asks_in():
        slots = asks.at[0 : n_kv - 1]
        return remote(slots, slots, ask_send.at[0], ask_recv.at[0], "kv", origin[1])

    def pair_part(j):
        block = pair_own[...] if j == 0 else pair_all[origin[j]]
        block = jnp.concatenate([block[k] for k in range(n_dp)], axis=1)
        return lax.dot_general(
            token_part(j), block, (((1,), (1,)), ((), ())), preferred_element_type=jnp.float32
        )

    def pair_stage():
        total = pair_part(0)
        for j in range(1, n_kv):
            total += pair_part(j)
        kv_own[...] = total.astype(jnp.bfloat16).reshape(blocks, BLOCK_LENGTH, LANES)

    def named(rows_of, owner):
        local = rows_of - owner * blocks
        inside = (local >= 0) & (local < blocks)
        return (
            jnp.min(jnp.where(inside, local, blocks - 1)),
            jnp.max(jnp.where(inside, local, 0)),
        )

    def kv_out(j):
        return remote(
            packed.at[j], kv_far.at[pl.ds(z * CAP, CAP)], kv_send.at[0], kv_recv.at[0],
            "kv", origin[j],
        )

    def kv_in():
        slots = kv_far.at[0 : (n_kv - 1) * CAP]
        return remote(slots, slots, kv_send.at[0], kv_recv.at[0], "kv", origin[1])

    picks = chosen.shape[1]

    def locate(b, carry):
        for s in range(picks):
            name = jnp.maximum(chosen[b, s], 0)
            owner = lax.div(name, blocks)
            far = owner * CAP + jnp.where(name == lowest_of[owner], 0, 1)
            spots[b, s] = jnp.where(owner == z, name - z * blocks + n_kv * CAP, far)
        return carry

    def share_blocks():
        kv_far[pl.ds(z * CAP, CAP)] = jnp.zeros((CAP, BLOCK_LENGTH, LANES), jnp.bfloat16)
        asks_in().wait_recv()
        for j in range(1, n_kv):
            lowest, highest = named(asks[origin[j]], z)
            packed[j, 0] = kv_own[lowest]
            packed[j, 1] = kv_own[highest]
        for owner in range(n_kv):
            lowest_of[owner] = named(wanted[...], owner)[0] + owner * blocks
        for j in range(1, n_kv):
            kv_out(j).start()
        lax.fori_loop(0, blocks, locate, 0)

    def query_part(part, j):
        term = jnp.dot(
            token_part(j), whole(1, j, part), preferred_element_type=jnp.float32
        )
        query_sum[...] = term if j == 0 else query_sum[...] + term

    heads = query_rows.shape[0]
    group = heads // PIECES[1]

    def query_tiles(part):
        low_half = lax.broadcasted_iota(jnp.int32, (rows, LANES), 1) < HEAD_WIDTH
        for p in range(group // 2):
            both = query_sum[:, p * LANES : (p + 1) * LANES]
            for side, one in enumerate((both, pltpu.roll(both, HEAD_WIDTH, 1))):
                one = jnp.where(low_half, one, 0.0).astype(jnp.bfloat16)
                one = one * jnp.bfloat16(HEAD_WIDTH ** (-0.5))
                query_rows[part * group + 2 * p + side] = one

    def gather_blocks():
        kv_in().wait_recv()
        kv_all[0 : n_kv * CAP] = kv_far[...]
        kv_all[n_kv * CAP :] = kv_own[...]

    lane = lax.broadcasted_iota(jnp.int32, (BLOCK_LENGTH, LANES), 1)
    row = lax.broadcasted_iota(jnp.int32, (BLOCK_LENGTH, LANES), 0)
    low = lane < HEAD_WIDTH

    def attend(part, start, count):
        def score(b):
            kv = jnp.concatenate([kv_all[spots[b, s]] for s in range(picks)], axis=0)
            query = query_rows[
                part * group : (part + 1) * group, b * BLOCK_LENGTH : (b + 1) * BLOCK_LENGTH, :
            ].reshape(group * BLOCK_LENGTH, LANES)
            scores = lax.dot_general(
                query, kv, (((1,), (1,)), ((), ())), preferred_element_type=jnp.float32
            )
            return kv, scores

        later = score(start)
        for b in range(start, start + count):
            kv, scores = later
            if b + 1 < start + count:
                later = score(b + 1)
            offs = [jnp.where(chosen[b, s] >= 0, 0.0, HIDDEN) for s in range(picks)]
            bias = []
            for s in range(0, picks, 2):
                tile = jnp.where(low, offs[s], offs[s + 1])
                if s == 0:
                    tile = jnp.where(low & (lane > row), HIDDEN, tile)
                bias.append(tile)
            bias = jnp.concatenate(bias, axis=1)
            scores = scores.reshape(group, BLOCK_LENGTH, picks * BLOCK_LENGTH) + bias[None]
            top = jnp.max(scores, axis=2, keepdims=True)
            expon = jnp.exp(scores - top)
            inverse = 1.0 / jnp.sum(expon, axis=2, keepdims=True)
            probs = expon.astype(jnp.bfloat16).reshape(group * BLOCK_LENGTH, picks * BLOCK_LENGTH)
            mixed = jnp.dot(probs, kv, preferred_element_type=jnp.float32)
            mixed = mixed.reshape(group, BLOCK_LENGTH, LANES) * inverse
            for p in range(group // 2):
                joined = jnp.where(low, pltpu.roll(mixed[2 * p], HEAD_WIDTH, 1), mixed[2 * p + 1])
                column = (part * group // 2 + p) * LANES
                attended[b * BLOCK_LENGTH : (b + 1) * BLOCK_LENGTH, column : column + LANES] = (
                    joined.astype(jnp.bfloat16)
                )

    loads[3].wait()
    for j in range(1, n_kv):
        ask(j).start()
    pltpu.make_async_copy(pair_own, pair_own, load_sem.at[5]).wait()
    out(1)
    query_loads[1].wait()
    for e in (6, 2, 0):
        out(e)
    query_loads[0].wait()
    for e in (4, 5):
        out(e)
    for e in (1, 6, 0):
        pass_on(e)
    out(3)
    pass_on(2)
    out(7)
    pass_on(4)
    relay(0)
    pass_on(3)
    relay(1)
    loads[1].wait()
    for e in (10, 12, 8):
        out(e)
    relay(2)
    out(13)
    relay(4)
    for e in (5, 7):
        pass_on(e)
    take(1)
    relay(3)
    for e in (0, 2):
        take(e)
    loads[0].wait()
    query_part(0, 0)
    pair_stage()
    loads[4].wait()
    share_blocks()
    for e in (5, 6):
        relay(e)
    pass_on(8)
    out(9)
    relay(7)
    for e in (10, 13):
        pass_on(e)
    take(3)
    query_part(0, 1)
    out(11)
    take(4)
    out(14)
    take(5)
    query_part(0, 2)
    query_part(0, 3)
    take(6)
    out_far(12)
    query_tiles(0)
    query_part(1, 0)
    query_part(1, 1)
    out_far(13)
    relay(8)
    gather_blocks()
    pass_on(9)
    attend(0, blocks * 0 // 2, blocks // 2)
    take(7)
    pass_on(11)
    attend(0, blocks * 1 // 2, blocks // 2)
    relay(10)
    query_part(1, 2)
    take(8)
    pass_on(12)
    query_part(1, 3)
    out_far(14)
    pass_far(12)
    query_tiles(1)
    relay(9)
    pass_far(13)
    pass_on(14)
    relay(13)
    attend(1, blocks * 0 // 2, blocks // 2)
    relay(11)
    attend(1, blocks * 1 // 2, blocks // 2)
    loads[2].wait()

    peer = lax.rem(t + 1, n_tp)
    other_rows = attended[pl.ds(pl.multiple_of(peer * half, half), half), :]
    own_rows = attended[pl.ds(pl.multiple_of(t * half, half), half), :]

    def swap_half(j):
        return remote(
            leaving.at[origin[j]], arriving.at[origin[j]], t_send.at[0], t_recv.at[j], "tp", peer
        )

    def project(j):
        weight = whole(2, j)
        leaving[origin[j]] = jnp.dot(
            other_rows, weight, preferred_element_type=jnp.float32
        ).astype(jnp.bfloat16)
        swap_half(j).start()
        kept[origin[j]] = jnp.dot(own_rows, weight, preferred_element_type=jnp.float32)

    pass_far(14)
    project(0)
    take(10)
    relay(12)
    take(9)
    project(1)
    relay(14)
    project(2)
    take(11)
    project(3)

    square = jnp.zeros((half, 1), jnp.float32)
    for j in range(n_kv):
        slot = origin[j]
        swap_half(j).wait_recv()
        mixed = kept[slot] + arriving[slot].astype(jnp.float32)
        kept[slot] = mixed
        square += jnp.sum(mixed * mixed, axis=1, keepdims=True)
    scale = lax.rsqrt(square * (1.0 / width) + 1e-06)
    for j in range(n_kv):
        columns = slice(j * depth, (j + 1) * depth)
        result[:, columns] = (kept[j] * scale * gain[:, columns]).astype(jnp.bfloat16)

    def drain(slots, sem):
        remote(slots, slots, sem, z_recv.at[0], "kv", origin[1]).wait_send()

    edge = out_all.shape[2] // PIECES[2] * (PIECES[2] - FAR)
    drain(pair_all.at[0 : n_kv - 1, 0:2], d_send.at[0])
    drain(query_all.at[0 : n_kv - 1, :, 0:2], d_send.at[1])
    drain(out_all.at[0 : n_kv - 1, 0:2], d_send.at[2])
    drain(pair_all.at[0 : n_kv - 1, 0], r_send.at[0])
    drain(query_all.at[0 : n_kv - 1, :, 0], r_send.at[1])
    if edge:
        drain(out_all.at[0 : n_kv - 1, 0, 0:edge], r_send.at[2])

    def drain_planes(planes):
        drain(pair_all.at[0:planes, 0], z_send.at[0])
        drain(query_all.at[0:planes, :, 0], z_send.at[1])
        drain(out_all.at[0:planes, 0], z_send.at[2])
        if FAR:
            drain(out_all.at[0:planes, 0, edge:], c_send.at[0])

    @pl.when(middle)
    def _():
        drain_planes(n_kv)

    @pl.when(jnp.logical_not(middle))
    def _():
        drain_planes(n_kv - 2)

    drain(packed.at[1:n_kv], kv_send.at[0])
    drain(asks.at[0 : n_kv - 1], ask_send.at[0])
    drain(leaving, t_send.at[0])


def per_device_fused(
    n_dp, n_kv, n_tp,
    tokens, chosen, query_weight, key_matrix, value_matrix, out_weight, out_gain,
):
    rows, width = tokens.shape
    depth, columns = query_weight.shape
    blocks = rows // BLOCK_LENGTH
    cut = lambda w: w.reshape(n_dp, w.shape[0] // n_dp, w.shape[1])
    query, out = cut(query_weight), cut(out_weight)
    pair = jax.ShapeDtypeStruct((n_dp, LANES, depth // n_dp), jnp.bfloat16)
    bf16, f32 = jnp.bfloat16, jnp.float32
    vmem = pl.BlockSpec(memory_space=pltpu.VMEM)
    off_core = pl.BlockSpec(memory_space=pltpu.HBM)
    dma = pltpu.SemaphoreType.DMA
    copies = sum(PIECES) * (n_kv - 1)
    return pl.pallas_call(
        functools.partial(fused, n_dp, n_kv, n_tp),
        out_shape=pltpu.VMEM((rows // n_tp, width), bf16),
        in_specs=[
            off_core, off_core, off_core, off_core, off_core, off_core, off_core,
        ],
        out_specs=vmem,
        scratch_shapes=[
            pltpu.SMEM((blocks, chosen.shape[1]), jnp.int32),
            pltpu.SMEM((blocks, chosen.shape[1]), jnp.int32),
            pltpu.SMEM((n_kv,), jnp.int32),
            pltpu.VMEM((1, width), f32),
            pltpu.VMEM((rows, width), bf16),
            pltpu.VMEM(pair.shape, bf16),
            pltpu.VMEM((PIECES[1],) + query.shape[:2] + (columns // PIECES[1],), bf16),
            pltpu.VMEM(out.shape, bf16),
            pltpu.VMEM((blocks, chosen.shape[1]), jnp.int32),
            pltpu.VMEM((n_kv, blocks, chosen.shape[1]), jnp.int32),
            pltpu.VMEM((n_kv, CAP, BLOCK_LENGTH, LANES), bf16),
            pltpu.VMEM((blocks, BLOCK_LENGTH, LANES), bf16),
            pltpu.VMEM((n_kv * CAP, BLOCK_LENGTH, LANES), bf16),
            pltpu.VMEM((n_kv,) + pair.shape, bf16),
            pltpu.VMEM(
                (n_kv, PIECES[1]) + query.shape[:2] + (columns // PIECES[1],), bf16
            ),
            pltpu.VMEM((n_kv,) + out.shape, bf16),
            pltpu.VMEM((n_kv * CAP + blocks, BLOCK_LENGTH, LANES), bf16),
            pltpu.VMEM((rows, columns // PIECES[1]), f32),
            pltpu.VMEM((columns // HEAD_WIDTH, rows, LANES), bf16),
            pltpu.VMEM((rows, columns), bf16),
            pltpu.VMEM((n_kv, rows // n_tp, width // n_kv), bf16),
            pltpu.VMEM((n_kv, rows // n_tp, width // n_kv), bf16),
            pltpu.VMEM((n_kv, rows // n_tp, width // n_kv), f32),
            dma((6 + PIECES[1],)), dma((3,)), dma((copies,)), dma((1,)), dma((max(1, FAR * (n_kv - 1)),)),
            dma((3,)), dma((copies,)), dma((3,)), dma((copies,)),
            dma((1,)), dma((1,)), dma((1,)), dma((n_kv,)), dma((1,)), dma((1,)),
        ],
        compiler_params=pltpu.CompilerParams(
            collective_id=0, has_side_effects=True, vmem_limit_bytes=54 * 1024 * 1024
        ),
    )(chosen, tokens, key_matrix.T, value_matrix.T, query, out, out_gain.reshape(1, width))


def per_device(tokens, chosen, query_weight, key_matrix, value_matrix, out_weight, out_gain):
    tok_rows = tokens.shape[0]
    blocks = tok_rows // BLOCK_LENGTH
    device = lax.axis_index("kv")
    kv_count = lax.axis_size("kv")
    whole_query, whole_key, whole_value = (
        lax.all_gather(query_weight, "kv", axis=0, tiled=True),
        lax.all_gather(key_matrix, "kv", axis=0, tiled=True),
        lax.all_gather(value_matrix, "kv", axis=0, tiled=True),
    )
    query_rows = jnp.dot(tokens, whole_query, preferred_element_type=jnp.float32).astype(
        jnp.bfloat16
    )
    key_rows = jnp.dot(tokens, whole_key, preferred_element_type=jnp.float32).astype(jnp.bfloat16)
    value_rows = jnp.dot(tokens, whole_value, preferred_element_type=jnp.float32).astype(
        jnp.bfloat16
    )
    paired = jnp.concatenate([key_rows, value_rows], axis=1)
    pair_width = paired.shape[1]
    safe_ids = jnp.maximum(chosen, 0)
    everyone = lax.all_gather(paired, "kv", axis=0, tiled=True).reshape(
        kv_count * blocks, BLOCK_LENGTH, pair_width
    )
    picked = jnp.take(everyone, safe_ids, axis=0)
    head_count = query_rows.shape[1] // HEAD_WIDTH
    grouped = query_rows.reshape(blocks, BLOCK_LENGTH, head_count, HEAD_WIDTH)
    offsets = jnp.arange(BLOCK_LENGTH, dtype=jnp.int32)
    query_pos = (device * blocks + jnp.arange(blocks, dtype=jnp.int32))[
        :, None
    ] * BLOCK_LENGTH + offsets[None, :]
    key_pos = safe_ids[:, :, None] * BLOCK_LENGTH + offsets[None, None, :]
    visible = (chosen >= 0)[:, None, :, None] & (
        key_pos[:, None, :, :] <= query_pos[:, :, None, None]
    )

    def attend_block(inputs):
        query_block, pair_block, seen = inputs
        block_keys = pair_block[..., :HEAD_WIDTH]
        block_values = pair_block[..., HEAD_WIDTH:]
        scores = jnp.einsum(
            "qgd,skd->gqsk", query_block, block_keys, preferred_element_type=jnp.float32
        ) * HEAD_WIDTH ** (-0.5)
        scores = jnp.where(seen[None], scores, -1e30)
        row_max = jnp.max(scores, axis=(2, 3), keepdims=True)
        expon = jnp.exp(scores - row_max)
        row_sum = jnp.sum(expon, axis=(2, 3), keepdims=True)
        weights_bf = (expon / row_sum).astype(jnp.bfloat16)
        result = jnp.einsum(
            "gqsk,skd->qgd", weights_bf, block_values, preferred_element_type=jnp.float32
        )
        return result.astype(jnp.bfloat16)

    attended = lax.map(attend_block, (grouped, picked, visible))
    attended = attended.reshape(tok_rows, head_count * HEAD_WIDTH)
    whole_out = lax.all_gather(out_weight, "kv", axis=1, tiled=True)
    mixed = lax.psum_scatter(
        jnp.dot(attended, whole_out, preferred_element_type=jnp.float32).astype(jnp.bfloat16),
        "tp",
        scatter_dimension=0,
        tiled=True,
    ).astype(jnp.float32)
    normed = mixed * lax.rsqrt(jnp.mean(mixed * mixed, axis=-1, keepdims=True) + 1e-06) * out_gain
    return normed.astype(jnp.bfloat16)


def solution(mesh):
    placed = (
        P(("dp", "kv"), None),
        P(("dp", "kv"), None),
        P("kv", "tp"),
        P("kv", "tp"),
        P("kv", "tp"),
        P("tp", "kv"),
        P(),
    )
    n_dp, n_kv, n_tp = (mesh.shape[name] for name in ("dp", "kv", "tp"))

    def body(tokens, chosen, query_weight, key_matrix, value_matrix, out_weight, out_gain):
        args = (tokens, chosen, query_weight, key_matrix, value_matrix, out_weight, out_gain)
        depth, columns = query_weight.shape
        whole_tiles = (
            depth % (LANES * n_dp) == 0
            and columns % (2 * LANES * PIECES[1]) == 0
            and columns % (2 * LANES * PIECES[1]) == 0
            and out_weight.shape[0] % (32 * PIECES[2] * n_dp) == 0
            and out_weight.shape[1] % LANES == 0
            and columns % LANES == 0
            and key_matrix.shape[1] == HEAD_WIDTH
            and chosen.shape[1] % 2 == 0
            and n_tp == 2
            and n_dp == 4
            and n_kv == 4
            and tokens.shape[0] == 8 * BLOCK_LENGTH
        )
        if whole_tiles:
            return per_device_fused(n_dp, n_kv, n_tp, *args)
        return per_device(*args)

    return jax.shard_map(
        body,
        mesh=mesh,
        in_specs=placed,
        out_specs=P(("dp", "kv", "tp"), None),
        check_vma=False,
    )
```

time: 45.3 us -> 42.3 us (0.934)
  Pallas kernels: 44.2 us -> 41.2 us
    pallas_call x1, Pallas kernels: 44.2 us -> 41.2 us  [per_device_fused(): pl.pallas_call(functools.partial(fused, n_dp, n_kv, n_tp), out_shape=pltp...]
where the time goes in v3:
time: 42.3 us; the launch traced here: 42.1 us
  Pallas kernels  41.2 us (97%)
  local copies, waits for them, and re-layouts  0.97 us (2%)
    pallas_call x1, Pallas kernels, per_device_fused(): pl.pallas_call(functools.partial(fused, n_dp, n_kv, n_tp), out_shape=pltp...  41.2 us
    unnamed x1, local copies, waits for them, and re-layouts  0.97 us

profile of v3, /device:TPU:1, one launch (start us, length us, event | category | flops | bytes accessed | tf_op | source)
XLA Modules:
  0.0 42.1 jit_solution(14450163041568707980)
XLA Ops:
  0.0 41.2 %shard_map.73 = bf16[256,2048]{1,0:T(8,128)(2,1)S(1)} custom-call(s32[8,16]{1,0:T(8,128)} %chosen_hbm.1, bf16[512,2048]{1,0:T(8,128)(2,1)} %tokens_hbm.1, bf16[64,512]{1,0:T(8,128)(2,1)} %bitcast.7, bf16[64,512]{1,0:T(8,128)(2,1)} %bitcast.8, bf16[4,128,512]{2,1,0:T(8,128)(2,1)} %bitcast.5, bf16[4,128,512]{2,1,0:T(8,128)(2,1)} %bitcast.6, f32[1,2048]{1,0:T(1,128)} %bitcast.9), custom_call_target="tpu_custom_call" | custom-call | tf_op jit(solution)/shard_map/pallas_call | solution.py:492
  41.2 1.0 %copy.9 = bf16[256,2048]{1,0:T(8,128)(2,1)} copy(bf16[256,2048]{1,0:T(8,128)(2,1)S(1)} %shard_map.73) | data formatting | bytes 2097152

commit v4 on v3

--- a/solution.py
+++ b/solution.py
@@ -30,8 +30,8 @@
 def fused(
     n_dp, n_kv, n_tp,
     chosen_hbm, tokens_hbm, key_hbm, value_hbm, query_hbm, out_hbm, gain_hbm, result,
-    chosen, spots, lowest_of, gain, tokens, pair_own, query_own, out_own, wanted, asks, packed, kv_own, kv_far,
-    pair_all, query_all, out_all, kv_all, query_sum, query_rows, attended,
+    chosen, spots, lowest_of, picked, gain, tokens, pair_own, query_own, out_own, wanted, asks, packed, kv_own, kv_far,
+    pair_all, query_all, out_all, keys, values, query_sum, query_rows, attended,
     leaving, arriving, kept,
     load_sem, z_send, z_recv, c_send, c_recv, d_send, d_recv, r_send, r_recv, kv_send, kv_recv, t_send, t_recv, ask_send, ask_recv,
 ):
@@ -228,32 +228,49 @@
             "kv", origin[j],
         )
 
-    def kv_in():
-        slots = kv_far.at[0 : (n_kv - 1) * CAP]
+    def kv_in(count):
+        slots = kv_far.at[0 : count * CAP]
         return remote(slots, slots, kv_send.at[0], kv_recv.at[0], "kv", origin[1])
 
+    later_peer = (None, lax.rem(z, 2) == 0, z < 2, z < 2)
+
     picks = chosen.shape[1]
+
+    absent = n_kv * CAP + blocks
 
     def locate(b, carry):
         for s in range(picks):
             name = jnp.maximum(chosen[b, s], 0)
             owner = lax.div(name, blocks)
             far = owner * CAP + jnp.where(name == lowest_of[owner], 0, 1)
-            spots[b, s] = jnp.where(owner == z, name - z * blocks + n_kv * CAP, far)
+            here = jnp.where(owner == z, name - z * blocks + n_kv * CAP, far)
+            spots[b, s] = jnp.where(chosen[b, s] >= 0, here, absent)
         return carry
 
-    def share_blocks():
-        kv_far[pl.ds(z * CAP, CAP)] = jnp.zeros((CAP, BLOCK_LENGTH, LANES), jnp.bfloat16)
+    def plan_blocks():
+        for owner in range(n_kv):
+
+            @pl.when(z <= owner)
+            def _(owner=owner):
+                kv_far[owner * CAP : (owner + 1) * CAP] = jnp.zeros(
+                    (CAP, BLOCK_LENGTH, LANES), jnp.bfloat16
+                )
+
+        for owner in range(n_kv):
+            lowest_of[owner] = named(wanted[...], owner)[0] + owner * blocks
+        lax.fori_loop(0, blocks, locate, 0)
         asks_in().wait_recv()
         for j in range(1, n_kv):
-            lowest, highest = named(asks[origin[j]], z)
-            packed[j, 0] = kv_own[lowest]
-            packed[j, 1] = kv_own[highest]
-        for owner in range(n_kv):
-            lowest_of[owner] = named(wanted[...], owner)[0] + owner * blocks
+            picked[j, 0], picked[j, 1] = named(asks[origin[j]], z)
+
+    def share_blocks():
         for j in range(1, n_kv):
-            kv_out(j).start()
-        lax.fori_loop(0, blocks, locate, 0)
+            for side in range(2):
+                packed[j, side] = kv_own[picked[j, side]]
+
+            @pl.when(later_peer[j])
+            def _(j=j):
+                kv_out(j).start()
 
     def query_part(part, j):
         term = jnp.dot(
@@ -265,56 +282,72 @@
     group = heads // PIECES[1]
 
     def query_tiles(part):
-        low_half = lax.broadcasted_iota(jnp.int32, (rows, LANES), 1) < HEAD_WIDTH
+        spread = lax.broadcasted_iota(jnp.int32, (rows, LANES), 1)
+        at_head = spread < HEAD_WIDTH
+        flag = jnp.where(spread == HEAD_WIDTH, 1.0, 0.0)
         for p in range(group // 2):
             both = query_sum[:, p * LANES : (p + 1) * LANES]
             for side, one in enumerate((both, pltpu.roll(both, HEAD_WIDTH, 1))):
-                one = jnp.where(low_half, one, 0.0).astype(jnp.bfloat16)
-                one = one * jnp.bfloat16(HEAD_WIDTH ** (-0.5))
-                query_rows[part * group + 2 * p + side] = one
-
-    def gather_blocks():
-        kv_in().wait_recv()
-        kv_all[0 : n_kv * CAP] = kv_far[...]
-        kv_all[n_kv * CAP :] = kv_own[...]
+                one = one.astype(jnp.bfloat16) * jnp.bfloat16(HEAD_WIDTH ** (-0.5))
+                query_rows[part * group + 2 * p + side] = jnp.where(
+                    at_head, one.astype(jnp.float32), flag
+                ).astype(jnp.bfloat16)
 
     lane = lax.broadcasted_iota(jnp.int32, (BLOCK_LENGTH, LANES), 1)
     row = lax.broadcasted_iota(jnp.int32, (BLOCK_LENGTH, LANES), 0)
     low = lane < HEAD_WIDTH
+    later_keys = jnp.where(low & (lane > row), HIDDEN, 0.0)
+
+    def gather_blocks():
+        for count in range(1, n_kv):
+
+            @pl.when(z == count)
+            def _(count=count):
+                kv_in(count).wait_recv()
+
+        for source, start in ((kv_far, 0), (kv_own, n_kv * CAP)):
+            both = source[...].astype(jnp.float32)
+            left = lax.broadcasted_iota(jnp.int32, both.shape, 2) < HEAD_WIDTH
+            keys[start : start + both.shape[0]] = jnp.where(left, both, 0.0).astype(jnp.bfloat16)
+            values[start : start + both.shape[0]] = jnp.where(left, 1.0, both).astype(jnp.bfloat16)
+        keys[absent] = jnp.where(lane == HEAD_WIDTH, HIDDEN, 0.0).astype(jnp.bfloat16)
+        values[absent] = jnp.zeros((BLOCK_LENGTH, LANES), jnp.bfloat16)
+
+    def chosen_rows(source, b):
+        return jnp.concatenate([source[spots[b, s]] for s in range(picks)], axis=0)
+
+    def score(part, b):
+        query = query_rows[
+            part * group : (part + 1) * group, b * BLOCK_LENGTH : (b + 1) * BLOCK_LENGTH, :
+        ].reshape(group * BLOCK_LENGTH, LANES)
+        return lax.dot_general(
+            query, chosen_rows(keys, b), (((1,), (1,)), ((), ())),
+            preferred_element_type=jnp.float32,
+        )
+
+    ahead = []
 
     def attend(part, start, count):
-        def score(b):
-            kv = jnp.concatenate([kv_all[spots[b, s]] for s in range(picks)], axis=0)
-            query = query_rows[
-                part * group : (part + 1) * group, b * BLOCK_LENGTH : (b + 1) * BLOCK_LENGTH, :
-            ].reshape(group * BLOCK_LENGTH, LANES)
-            scores = lax.dot_general(
-                query, kv, (((1,), (1,)), ((), ())), preferred_element_type=jnp.float32
+        for b in range(start, start + count):
+            scores = ahead.pop() if ahead else score(part, b)
+            if b + 1 < blocks:
+                ahead.append(score(part, b + 1))
+            scores = scores.reshape(group, BLOCK_LENGTH, picks * BLOCK_LENGTH)
+            head, rest = scores[:, :, :LANES] + later_keys[None], scores[:, :, LANES:]
+            top = jnp.maximum(
+                jnp.max(head, axis=2, keepdims=True), jnp.max(rest, axis=2, keepdims=True)
             )
-            return kv, scores
-
-        later = score(start)
-        for b in range(start, start + count):
-            kv, scores = later
-            if b + 1 < start + count:
-                later = score(b + 1)
-            offs = [jnp.where(chosen[b, s] >= 0, 0.0, HIDDEN) for s in range(picks)]
-            bias = []
-            for s in range(0, picks, 2):
-                tile = jnp.where(low, offs[s], offs[s + 1])
-                if s == 0:
-                    tile = jnp.where(low & (lane > row), HIDDEN, tile)
-                bias.append(tile)
-            bias = jnp.concatenate(bias, axis=1)
-            scores = scores.reshape(group, BLOCK_LENGTH, picks * BLOCK_LENGTH) + bias[None]
-            top = jnp.max(scores, axis=2, keepdims=True)
-            expon = jnp.exp(scores - top)
-            inverse = 1.0 / jnp.sum(expon, axis=2, keepdims=True)
+            expon = jnp.concatenate([jnp.exp(head - top), jnp.exp(rest - top)], axis=2)
             probs = expon.astype(jnp.bfloat16).reshape(group * BLOCK_LENGTH, picks * BLOCK_LENGTH)
-            mixed = jnp.dot(probs, kv, preferred_element_type=jnp.float32)
-            mixed = mixed.reshape(group, BLOCK_LENGTH, LANES) * inverse
+            mixed = jnp.dot(probs, chosen_rows(values, b), preferred_element_type=jnp.float32)
+            mixed = mixed.reshape(group, BLOCK_LENGTH, LANES)
             for p in range(group // 2):
-                joined = jnp.where(low, pltpu.roll(mixed[2 * p], HEAD_WIDTH, 1), mixed[2 * p + 1])
+                even, odd = mixed[2 * p], mixed[2 * p + 1]
+                joined = jnp.where(
+                    low,
+                    pltpu.roll(even, HEAD_WIDTH, 1) / even,
+                    odd / pltpu.roll(odd, HEAD_WIDTH, 1),
+                )
                 column = (part * group // 2 + p) * LANES
                 attended[b * BLOCK_LENGTH : (b + 1) * BLOCK_LENGTH, column : column + LANES] = (
                     joined.astype(jnp.bfloat16)
@@ -334,6 +367,8 @@
     for e in (1, 6, 0):
         pass_on(e)
     out(3)
+    loads[4].wait()
+    plan_blocks()
     pass_on(2)
     out(7)
     pass_on(4)
@@ -345,58 +380,55 @@
         out(e)
     relay(2)
     out(13)
-    relay(4)
     for e in (5, 7):
         pass_on(e)
     take(1)
     relay(3)
-    for e in (0, 2):
-        take(e)
+    take(0)
+    relay(4)
+    take(2)
     loads[0].wait()
-    query_part(0, 0)
     pair_stage()
-    loads[4].wait()
     share_blocks()
     for e in (5, 6):
         relay(e)
     pass_on(8)
     out(9)
+    pass_on(10)
+    query_part(0, 0)
+    take(3)
     relay(7)
-    for e in (10, 13):
-        pass_on(e)
-    take(3)
-    query_part(0, 1)
     out(11)
     take(4)
-    out(14)
+    query_part(0, 1)
     take(5)
     query_part(0, 2)
     query_part(0, 3)
-    take(6)
     out_far(12)
+    out(14)
     query_tiles(0)
-    query_part(1, 0)
-    query_part(1, 1)
     out_far(13)
-    relay(8)
     gather_blocks()
     pass_on(9)
     attend(0, blocks * 0 // 2, blocks // 2)
+    relay(8)
+    pass_on(13)
+    take(6)
+    query_part(1, 0)
+    query_part(1, 1)
     take(7)
+    attend(0, blocks * 1 // 2, blocks // 2)
     pass_on(11)
-    attend(0, blocks * 1 // 2, blocks // 2)
+    out_far(14)
     relay(10)
     query_part(1, 2)
     take(8)
     pass_on(12)
     query_part(1, 3)
-    out_far(14)
-    pass_far(12)
+    pass_on(14)
     query_tiles(1)
     relay(9)
     pass_far(13)
-    pass_on(14)
-    relay(13)
     attend(1, blocks * 0 // 2, blocks // 2)
     relay(11)
     attend(1, blocks * 1 // 2, blocks // 2)
@@ -419,7 +451,9 @@
         swap_half(j).start()
         kept[origin[j]] = jnp.dot(own_rows, weight, preferred_element_type=jnp.float32)
 
-    pass_far(14)
+    relay(13)
+    for e in (12, 14):
+        pass_far(e)
     project(0)
     take(10)
     relay(12)
@@ -469,7 +503,12 @@
     def _():
         drain_planes(n_kv - 2)
 
-    drain(packed.at[1:n_kv], kv_send.at[0])
+    for count in range(1, n_kv):
+
+        @pl.when(z == n_kv - 1 - count)
+        def _(count=count):
+            drain(packed.at[1 : count + 1], kv_send.at[0])
+
     drain(asks.at[0 : n_kv - 1], ask_send.at[0])
     drain(leaving, t_send.at[0])
 
@@ -500,6 +539,7 @@
             pltpu.SMEM((blocks, chosen.shape[1]), jnp.int32),
             pltpu.SMEM((blocks, chosen.shape[1]), jnp.int32),
             pltpu.SMEM((n_kv,), jnp.int32),
+            pltpu.SMEM((n_kv, 2), jnp.int32),
             pltpu.VMEM((1, width), f32),
             pltpu.VMEM((rows, width), bf16),
             pltpu.VMEM(pair.shape, bf16),
@@ -515,7 +555,8 @@
                 (n_kv, PIECES[1]) + query.shape[:2] + (columns // PIECES[1],), bf16
             ),
             pltpu.VMEM((n_kv,) + out.shape, bf16),
-            pltpu.VMEM((n_kv * CAP + blocks, BLOCK_LENGTH, LANES), bf16),
+            pltpu.VMEM((n_kv * CAP + blocks + 1, BLOCK_LENGTH, LANES), bf16),
+            pltpu.VMEM((n_kv * CAP + blocks + 1, BLOCK_LENGTH, LANES), bf16),
             pltpu.VMEM((rows, columns // PIECES[1]), f32),
             pltpu.VMEM((columns // HEAD_WIDTH, rows, LANES), bf16),
             pltpu.VMEM((rows, columns), bf16),

time: 42.3 us -> 41.3 us (0.976)
  Pallas kernels: 41.2 us -> 40.2 us
    pallas_call x1, Pallas kernels: 41.2 us -> 40.2 us  [per_device_fused(): pl.pallas_call(functools.partial(fused, n_dp, n_kv, n_tp), out_shape=pltp...]
where the time goes in v4:
time: 41.3 us; the launch traced here: 41.2 us
  Pallas kernels  40.2 us (97%)
  local copies, waits for them, and re-layouts  0.97 us (2%)
    pallas_call x1, Pallas kernels, per_device_fused(): pl.pallas_call(functools.partial(fused, n_dp, n_kv, n_tp), out_shape=pltp...  40.2 us
    unnamed x1, local copies, waits for them, and re-layouts  0.97 us

profile of v4, /device:TPU:1, one launch (start us, length us, event | category | flops | bytes accessed | tf_op | source)
XLA Modules:
  0.0 41.2 jit_solution(9932212350900904629)
XLA Ops:
  0.0 40.2 %shard_map.73 = bf16[256,2048]{1,0:T(8,128)(2,1)S(1)} custom-call(s32[8,16]{1,0:T(8,128)} %chosen_hbm.1, bf16[512,2048]{1,0:T(8,128)(2,1)} %tokens_hbm.1, bf16[64,512]{1,0:T(8,128)(2,1)} %bitcast.7, bf16[64,512]{1,0:T(8,128)(2,1)} %bitcast.8, bf16[4,128,512]{2,1,0:T(8,128)(2,1)} %bitcast.5, bf16[4,128,512]{2,1,0:T(8,128)(2,1)} %bitcast.6, f32[1,2048]{1,0:T(1,128)} %bitcast.9), custom_call_target="tpu_custom_call" | custom-call | tf_op jit(solution)/shard_map/pallas_call | solution.py:531
  40.2 1.0 %copy.9 = bf16[256,2048]{1,0:T(8,128)(2,1)} copy(bf16[256,2048]{1,0:T(8,128)(2,1)S(1)} %shard_map.73) | data formatting | bytes 2097152

commit v5 on v4

--- a/solution.py
+++ b/solution.py
@@ -69,13 +69,13 @@
         load.start()
 
     barrier = pltpu.get_barrier_semaphore()
-    for axis, me, count in (("dp", d, n_dp), ("kv", z, n_kv), ("tp", t, n_tp)):
-        for step in range(1, count):
-            pl.semaphore_signal(
-                barrier, inc=1, device_id={axis: lax.rem(me + step, count)},
-                device_id_type=pl.DeviceIdType.MESH,
-            )
-    pl.semaphore_wait(barrier, n_dp + n_kv + n_tp - 3)
+    partners = [("kv", lax.rem(z + step, n_kv)) for step in range(1, n_kv)]
+    partners += [("dp", d + 1 - 2 * lax.rem(d, 2)), ("dp", lax.rem(d + 2, 4)), ("tp", 1 - t)]
+    for axis, partner in partners:
+        pl.semaphore_signal(
+            barrier, inc=1, device_id={axis: partner}, device_id_type=pl.DeviceIdType.MESH
+        )
+    pl.semaphore_wait(barrier, len(partners))
 
     owns = (pair_own, query_own, out_own)
     alls = (pair_all, query_all, out_all)

time: 41.3 us -> 41.2 us (level)
  no operation moved by 1% of the time
where the time goes in v5:
time: 41.2 us; the launch traced here: 41.1 us
  Pallas kernels  40.1 us (97%)
  local copies, waits for them, and re-layouts  0.97 us (2%)
    pallas_call x1, Pallas kernels, per_device_fused(): pl.pallas_call(functools.partial(fused, n_dp, n_kv, n_tp), out_shape=pltp...  40.1 us
    unnamed x1, local copies, waits for them, and re-layouts  0.97 us

profile of v5, /device:TPU:1, one launch (start us, length us, event | category | flops | bytes accessed | tf_op | source)
XLA Modules:
  0.0 41.1 jit_solution(7703537247613255300)
XLA Ops:
  0.0 40.1 %shard_map.73 = bf16[256,2048]{1,0:T(8,128)(2,1)S(1)} custom-call(s32[8,16]{1,0:T(8,128)} %chosen_hbm.1, bf16[512,2048]{1,0:T(8,128)(2,1)} %tokens_hbm.1, bf16[64,512]{1,0:T(8,128)(2,1)} %bitcast.7, bf16[64,512]{1,0:T(8,128)(2,1)} %bitcast.8, bf16[4,128,512]{2,1,0:T(8,128)(2,1)} %bitcast.5, bf16[4,128,512]{2,1,0:T(8,128)(2,1)} %bitcast.6, f32[1,2048]{1,0:T(1,128)} %bitcast.9), custom_call_target="tpu_custom_call" | custom-call | tf_op jit(solution)/shard_map/pallas_call | solution.py:531
  40.1 1.0 %copy.9 = bf16[256,2048]{1,0:T(8,128)(2,1)} copy(bf16[256,2048]{1,0:T(8,128)(2,1)S(1)} %shard_map.73) | data formatting | bytes 2097152
